TPU v7x, 256 devices: a whole 4x4x8 slice. The times are simulated.
256 devices in a mesh: sp: 64 (over z, x, core), tp: 4 (over y).
Axes of the slice: x: 4, y: 4, z: 8, core: 2. Of those that a mesh axis runs over, the one named last changes fastest.
Arguments:
- residual: bfloat16 [8192, 2048], P(('sp', 'tp')), may hold values from -6 to 6
- query_rows: bfloat16 [8192, 1024], P('sp', 'tp'), may hold values from -6 to 6
- key_rows: bfloat16 [8192, 512], P('sp', 'tp'), may hold values from -6 to 6
- value_rows: bfloat16 [8192, 512], P('sp', 'tp'), may hold values from -8 to 8
- head_offset: float32 [8], P('tp'), may hold values from -13 to -3
- w_out: bfloat16 [1024, 2048], P('tp'), may hold values from -0.5 to 0.5
- norm_gain: float32 [2, 2048], replicated, may hold values from 0.1 to 1.9
- norm_bias: float32 [2, 2048], replicated, may hold values from -1.5 to 1.5
- routing: int32 [8192, 2], P(('sp', 'tp')), may hold values from 0 to 63, all different within a row; in each aligned block of 32 rows (0 to 31, 32 to 63, ...) at most 2 rows name the same one
- route_weight: float32 [8192, 2], P(('sp', 'tp')), may hold values from 0.2 to 1
- w_exp_gate: bfloat16 [64, 2048, 1024], P('sp', None, 'tp'), may hold values from -0.125 to 0.125
- w_exp_up: bfloat16 [64, 2048, 1024], P('sp', None, 'tp'), may hold values from -0.125 to 0.125
- w_exp_down: bfloat16 [64, 1024, 2048], P('sp', 'tp'), may hold values from -0.1875 to 0.1875
- w_shared_gate: bfloat16 [2048, 1024], P(None, 'tp'), may hold values from -0.125 to 0.125
- w_shared_up: bfloat16 [2048, 1024], P(None, 'tp'), may hold values from -0.125 to 0.125
- w_shared_down: bfloat16 [1024, 2048], P('tp'), may hold values from -0.1875 to 0.1875
Outputs:
- result: bfloat16 [8192, 2048], P(('sp', 'tp'))
Inputs may be any that keep to these rules, and one draw needn't show every extreme that they name: `routing`: each row names 2 different experts; within the rows of one device (32 tokens) no expert is named by more than 2 of them, a bound that some block reaches.
All inputs are finite; a program needn't handle non-finite values.
Results may differ from a plain program's by a relative error of at most 0.013.
Values may be sent and summed in bfloat16 or wider, within the bound.
A program may use at most 64 MiB of HBM per device.

v0:
```python
import jax
import jax.numpy as jnp
from jax import lax
from jax.sharding import PartitionSpec as P

DH = 128


ALPHA = 8.0**0.25
LN_EPS = 1e-05


def in_one_piece(arrays, axis, dim, along):
    both = jnp.concatenate(arrays, axis=along)
    whole, at, done = (lax.all_gather(both, axis, axis=dim, tiled=True), 0, [])
    for a in arrays:
        done.append(lax.slice_in_dim(whole, at, at + a.shape[along], axis=along))
        at += a.shape[along]
    return tuple(done)


def split_up(array, dim, peers):
    dims = array.shape
    blocks = array.reshape(*dims[:dim], peers, dims[dim] // peers, *dims[dim + 1 :])
    return jnp.moveaxis(blocks, dim, 0)


def summed_on_arrival(array, axis, dim):
    peers = lax.axis_size(axis)
    blocks = lax.all_to_all(split_up(array, dim, peers), axis, 0, 0, tiled=True)
    return jnp.sum(blocks.astype(jnp.float32), axis=0)


def sent_to_all(array, axis):
    peers = lax.axis_size(axis)
    return lax.all_to_all(
        jnp.broadcast_to(array[None], (peers, *array.shape)), axis, 0, 0, tiled=True
    )


def joined_along(blocks, dim):
    dims = list(blocks.shape[1:])
    dims[dim] *= blocks.shape[0]
    return jnp.moveaxis(blocks, 0, dim).reshape(dims)


def collect(array, axis, dim):
    blocks = sent_to_all(array, axis)
    return joined_along(blocks, dim)


def layer_norm(summed, gain, shift):
    center = summed - jnp.mean(summed, axis=-1, keepdims=True)
    spread = jnp.mean(center * center, axis=-1, keepdims=True)
    return (center * lax.rsqrt(spread + LN_EPS) * gain + shift).astype(jnp.bfloat16)


def stick_terms(queries, keys_block, key_start, query_pos, offset, shard_len):
    kv_local, group_size = offset.shape
    query_count = queries.shape[0]
    key_count = keys_block.shape[0]
    head_dim = keys_block.shape[-1]
    scores = jnp.einsum("tkgd,skd->kgts", queries, keys_block, preferred_element_type=jnp.float32)
    scores = scores * head_dim ** (-0.5) + offset[:, :, None, None]
    key_pos = key_start + jnp.arange(key_count, dtype=jnp.int32)
    causal = key_pos[None, :] < query_pos[:, None]
    leftover = jnp.where(causal, jax.nn.log_sigmoid(-scores), 0.0)
    shape_five = (kv_local, group_size, query_count, key_count // shard_len, shard_len)
    causal = causal.reshape(query_count, key_count // shard_len, shard_len)
    return (scores.reshape(shape_five), causal, leftover.reshape(shape_five))


def stick_block(queries, keys_block, values_block, key_start, query_pos, offset, shard_len, beyond):
    scores, causal, leftover = stick_terms(
        queries, keys_block, key_start, query_pos, offset, shard_len
    )
    within = lax.cumsum(leftover, axis=4, reverse=True) - leftover
    totals = jnp.sum(leftover, axis=4)
    beyond = beyond + lax.cumsum(totals, axis=3, reverse=True) - totals
    exponent = jax.nn.log_sigmoid(scores) + within + beyond[..., None]
    weights = jnp.where(causal[None, None], jnp.exp(exponent), 0.0).astype(jnp.bfloat16)
    weights = weights.reshape(scores.shape[0], scores.shape[1], scores.shape[2], -1)
    partial_out = jnp.einsum(
        "kgts,skd->tkgd", weights, values_block, preferred_element_type=jnp.float32
    )
    return (partial_out, totals)


def per_device(
    residual,
    query_rows,
    key_rows,
    value_rows,
    head_offset,
    w_out,
    norm_gain,
    norm_bias,
    routing,
    route_weight,
    w_exp_gate,
    w_exp_up,
    w_exp_down,
    w_shared_gate,
    w_shared_up,
    w_shared_down,
):
    shard_len = query_rows.shape[0]
    kv_local = key_rows.shape[1] // DH
    heads_local = query_rows.shape[1] // DH
    group_size = heads_local // kv_local
    sp_count = lax.axis_size("sp")
    sp_index = lax.axis_index("sp")
    queries = query_rows.reshape(shard_len, kv_local, group_size, DH)
    offset = head_offset.reshape(kv_local, group_size)
    query_pos = sp_index * shard_len + jnp.arange(shard_len, dtype=jnp.int32)
    empty_out = jnp.zeros((shard_len, kv_local, group_size, DH), jnp.float32)
    all_keys, all_values = in_one_piece((key_rows, value_rows), "sp", 0, 1)
    all_keys = all_keys.reshape(-1, kv_local, DH)
    all_values = all_values.reshape(-1, kv_local, DH)
    turn_count = min(16, sp_count)
    block_len = shard_len * sp_count // turn_count
    own_block = sp_index * shard_len // block_len

    def turn(step_index, state_now):
        total_out, passed = state_now
        first_key = (own_block - step_index) * block_len
        keys_block = lax.dynamic_slice_in_dim(all_keys, first_key, block_len, 0)
        values_block = lax.dynamic_slice_in_dim(all_values, first_key, block_len, 0)
        beyond = jnp.broadcast_to(passed[..., None], passed.shape + (block_len // shard_len,))
        partial_out, totals = stick_block(
            queries, keys_block, values_block, first_key, query_pos, offset, shard_len, beyond
        )
        return (total_out + partial_out, passed + jnp.sum(totals, axis=3))

    start_state = (empty_out, jnp.zeros((kv_local, group_size, shard_len), jnp.float32))
    attended, _ = lax.fori_loop(0, own_block + 1, turn, start_state)
    attended = attended.astype(jnp.bfloat16).reshape(shard_len, heads_local * DH)
    rows_local = residual.shape[0]
    mixed = summed_on_arrival(
        jnp.dot(attended, w_out, preferred_element_type=jnp.float32).astype(jnp.bfloat16), "tp", 0
    )
    normed = layer_norm(ALPHA * residual.astype(jnp.float32) + mixed, norm_gain[0], norm_bias[0])
    top_k = routing.shape[1]
    exp_local = w_exp_gate.shape[0]
    experts = exp_local * sp_count
    capacity = max(2, 3 * rows_local * top_k // (2 * experts))
    flat_routes = routing.reshape(-1)
    one_hot = (flat_routes[:, None] == jnp.arange(experts, dtype=jnp.int32)[None, :]).astype(
        jnp.int32
    )
    slot_rank = jnp.sum((jnp.cumsum(one_hot, axis=0) - 1) * one_hot, axis=1)
    slot_index = flat_routes * capacity + slot_rank
    pair_token = jnp.arange(flat_routes.shape[0], dtype=jnp.int32) // top_k
    source_row = (
        jnp.full((experts * capacity,), rows_local, jnp.int32).at[slot_index].set(pair_token)
    )
    outgoing = jnp.take(normed, source_row, axis=0, mode="fill", fill_value=0)
    outgoing = outgoing.reshape(sp_count, exp_local, capacity, -1)
    arrived = lax.all_to_all(outgoing, "sp", split_axis=0, concat_axis=0, tiled=True)
    routed_rows, token_rows = (collect(arrived, "tp", 0), collect(normed, "tp", 0))
    gate_part = jnp.einsum(
        "aecd,edf->aecf", routed_rows, w_exp_gate, preferred_element_type=jnp.float32
    )
    up_part = jnp.einsum(
        "aecd,edf->aecf", routed_rows, w_exp_up, preferred_element_type=jnp.float32
    )
    hidden = (jax.nn.silu(gate_part) * up_part).astype(jnp.bfloat16)
    expert_part = jnp.einsum(
        "aecf,efd->aecd", hidden, w_exp_down, preferred_element_type=jnp.float32
    )
    shared_gate = jnp.dot(token_rows, w_shared_gate, preferred_element_type=jnp.float32)
    shared_up = jnp.dot(token_rows, w_shared_up, preferred_element_type=jnp.float32)
    shared_hidden = (jax.nn.silu(shared_gate) * shared_up).astype(jnp.bfloat16)
    shared_part = jnp.dot(shared_hidden, w_shared_down, preferred_element_type=jnp.float32)
    expert_sum, shared_sum = (
        summed_on_arrival(expert_part.astype(jnp.bfloat16), "tp", 0),
        summed_on_arrival(shared_part.astype(jnp.bfloat16), "tp", 0),
    )
    returned = lax.all_to_all(
        expert_sum.astype(jnp.bfloat16), "sp", split_axis=0, concat_axis=0, tiled=True
    )
    returned = returned.reshape(experts * capacity, -1)
    picked = returned[slot_index].astype(jnp.float32).reshape(rows_local, top_k, -1)
    routed = jnp.sum(picked * route_weight[:, :, None], axis=1)
    shared_out = lax.optimization_barrier(shared_sum.astype(jnp.bfloat16))
    combined = routed + shared_out.astype(jnp.float32)
    return layer_norm(ALPHA * normed.astype(jnp.float32) + combined, norm_gain[1], norm_bias[1])


def solution(mesh):
    placed = (
        P(("sp", "tp"), None),
        P("sp", "tp"),
        P("sp", "tp"),
        P("sp", "tp"),
        P("tp"),
        P("tp", None),
        P(),
        P(),
        P(("sp", "tp"), None),
        P(("sp", "tp"), None),
        P("sp", None, "tp"),
        P("sp", None, "tp"),
        P("sp", "tp", None),
        P(None, "tp"),
        P(None, "tp"),
        P("tp", None),
    )
    return jax.shard_map(
        per_device, mesh=mesh, in_specs=placed, out_specs=P(("sp", "tp"), None), check_vma=False
    )
```

profile of v0, /device:TPU:1, one launch (start us, length us, event | category | flops | bytes accessed | tf_op | source)
XLA Modules:
  0.0 356.5 jit_solution(12075126792649926036)
XLA Ops:
  6.5 1.5 pad_maximum_fusion
  13.1 80.2 %all-gather.2.cloned.1.call-done = bf16[8192,256]{1,0:T(8,128)(2,1)} async-done(((bf16[128,256]{1,0:T(8,128)(2,1)}), bf16[8192,256]{1,0:T(8,128)(2,1)}) %all-gather.2.cloned.1.call-update) | async-done | bytes 4194320 | tf_op jit(solution)/shard_map/all_gather | solution.py:15
  93.3 4.5 %slice_bitcast_fusion = (bf16[8192,1,128]{2,0,1:T(8,128)(2,1)}, bf16[8192,1,128]{2,0,1:T(8,128)(2,1)}) fusion(bf16[8192,256]{1,0:T(8,128)(2,1)} %all-gather.2.cloned.1.call-done), kind=kLoop, calls=%fused_computation.42 | loop fusion | bytes 8388608 | tf_op jit(solution)/shard_map/reshape | solution.py:118
  97.8 6.2 %while.13 = (s32[]{:T(128)}, f32[128,1,2,128]{0,3,2,1:T(8,128)S(1)}, f32[1,2,128]{2,1,0:T(2,128)S(1)}, s32[]{:T(128)}, s32[]{:T(128)}, /*index=5*/bf16[8192,1,12...) while((s32[]{:T(128)}, ...), condition=%wide.region_5.6_spmd.clone, body=%wide.region_0.5_spmd.clone.sunk | while | flops 88250504 | bytes 6203627 | solution.py:136
  98.1 1.5 fusion.75
  99.7 2.4 fusion.76
  105.2 4.0 %all-to-all-start = ((bf16[4,32,2048]{2,1,0:T(8,128)(2,1)}), bf16[4,32,2048]{2,1,0:T(8,128)(2,1)S(1)}, u32[]{:S(2)}, u32[]{:S(2)}) async-start(bf16[4,32,2048]{2,1,0:T(8,128)(2,1)} %bitcast.4), calls=%async_computation | async-start | bytes 1048576 | tf_op jit(solution)/shard_map/all_to_all | solution.py:30
  109.3 9.0 %all-to-all-done = bf16[4,32,2048]{2,1,0:T(8,128)(2,1)S(1)} async-done(((bf16[4,32,2048]{2,1,0:T(8,128)(2,1)}), bf16[4,32,2048]{2,1,0:T(8,128)(2,1)S(1)}, u32[]{:S(2)}, u32[]{:S(2)}) %all-to-all-start) | async-done | bytes 524320 | tf_op jit(solution)/shard_map/all_to_all | solution.py:30
  120.7 116.5 %all_to_all.35 = bf16[64,1,2,2048]{3,2,1,0:T(2,128)(2,1)S(1)} all-to-all(bf16[64,1,2,2048]{3,2,1,0:T(2,128)(2,1)S(1)} %broadcast_select_fusion), channel_id=1, replica_groups=mesh['sp'=64,'tp'=4] {'sp'}, dimensions={0} | all-to-all | bytes 1048576 | tf_op jit(solution)/shard_map/all_to_all | solution.py:159
  237.6 28.5 %all_to_all.36 = bf16[4,64,1,2,2048]{4,1,3,2,0:T(8,128)(2,1)S(1)} all-to-all(bf16[4,64,1,2,2048]{4,1,3,2,0:T(8,128)(2,1)S(1)} %broadcast_in_dim.80), channel_id=1, replica_groups=mesh['sp'=64,'tp'=4] {'tp'}, dimensions={0} | all-to-all | bytes 4194304 | tf_op jit(solution)/shard_map/all_to_all | solution.py:36
  267.0 4.3 %all-to-all-start.5 = ((bf16[4,32,2048]{2,1,0:T(8,128)(2,1)}), bf16[4,32,2048]{2,1,0:T(8,128)(2,1)}, u32[]{:S(2)}, u32[]{:S(2)}) async-start(bf16[4,32,2048]{2,1,0:T(8,128)(2,1)} %broadcast_in_dim.81), calls=%async_computation.5 | async-start | bytes 1048576 | tf_op jit(solution)/shard_map/all_to_all | solution.py:36
  271.5 1.3 copy-done.1
  272.9 1.5 convolution_bitcast_fusion.2
  274.4 4.3 %convolution_convert_fusion = bf16[256,2,2048]{2,0,1:T(8,128)(2,1)S(1)} fusion(bf16[256,2,2048]{2,0,1:T(8,128)(2,1)} %bitcast.148, bf16[1,256,2048]{2,1,0:T(8,128)(2,1)S(1)} %copy-done, bf16[1,2048,256]{2,1,0:T(8,128)(2,1)} %param.29, f32[256,1,2,256]{3,0,2,1:T(8,128)} %convolution_bitcast_fusion.2), kind=kOutput, calls=%fused_computation.39 | convolution fusion | flops 1075576832 | bytes 6815744 | tf_op jit(solution)/shard_map/aecf,efd->aecd/dot_general | solution.py:168
  278.7 1.5 copy.45
  280.2 4.0 %all-to-all-start.3 = ((bf16[4,64,1,2,2048]{4,1,3,2,0:T(8,128)(2,1)}), bf16[4,64,1,2,2048]{4,1,3,2,0:T(8,128)(2,1)S(1)}, u32[]{:S(2)}, u32[]{:S(2)}) async-start(bf16[4,64,1,2,2048]{4,1,3,2,0:T(8,128)(2,1)} %copy.45), calls=%async_computation.3 | async-start | bytes 4194304 | tf_op jit(solution)/shard_map/all_to_all | solution.py:30
  284.2 1.7 fusion.55
  285.9 3.3 convolution_convert_fusion.1
  289.2 19.6 %all-to-all-done.3 = bf16[4,64,1,2,2048]{4,1,3,2,0:T(8,128)(2,1)S(1)} async-done(((bf16[4,64,1,2,2048]{4,1,3,2,0:T(8,128)(2,1)}), bf16[4,64,1,2,2048]{4,1,3,2,0:T(8,128)(2,1)S(1)}, u32[]{:S(2)}, u32[]{:S(2)}) %all-to-all-start.3) | async-done | bytes 2097184 | tf_op jit(solution)/shard_map/all_to_all | solution.py:30
  308.8 4.1 %all-to-all-start.6 = ((bf16[4,32,2048]{2,1,0:T(8,128)(2,1)}), bf16[4,32,2048]{2,1,0:T(8,128)(2,1)}, u32[]{:S(2)}, u32[]{:S(2)}) async-start(bf16[4,32,2048]{2,1,0:T(8,128)(2,1)} %bitcast.146), calls=%async_computation.6 | async-start | bytes 1048576 | tf_op jit(solution)/shard_map/all_to_all | solution.py:30
  314.3 2.4 copy.47
  316.7 3.3 all-to-all-done.6
  320.0 8.8 %all-to-all-start.4 = ((bf16[64,1,2,2048]{3,2,1,0:T(2,128)(2,1)}), bf16[64,1,2,2048]{3,2,1,0:T(2,128)(2,1)S(1)}, u32[]{:S(2)}, u32[]{:S(2)}) async-start(bf16[64,1,2,2048]{3,2,1,0:T(2,128)(2,1)} %copy.47), calls=%async_computation.4 | async-start | bytes 1048576 | tf_op jit(solution)/shard_map/all_to_all | solution.py:179
  330.0 16.5 %all-to-all-done.4 = bf16[64,1,2,2048]{3,2,1,0:T(2,128)(2,1)S(1)} async-done(((bf16[64,1,2,2048]{3,2,1,0:T(2,128)(2,1)}), bf16[64,1,2,2048]{3,2,1,0:T(2,128)(2,1)S(1)}, u32[]{:S(2)}, u32[]{:S(2)}) %all-to-all-start.4) | async-done | bytes 524320 | tf_op jit(solution)/shard_map/all_to_all | solution.py:179
  (78 shorter events, 18.0 us)
Async XLA Ops:
  6.5 267.9 %copy-start = (bf16[1,256,2048]{2,1,0:T(8,128)(2,1)S(1)}, bf16[1,256,2048]{2,1,0:T(8,128)(2,1)}, u32[]{:S(2)}) copy-start(bf16[1,256,2048]{2,1,0:T(8,128)(2,1)} %param.30) | copy-start | bytes 3145732
  6.5 86.8 %all-gather.2.cloned.1.call-start = ((), (), s32[]{:S(2)}) async-start(), calls=%async_computation.7 | async-start | bytes 4259840 | tf_op jit(solution)/shard_map/all_gather | solution.py:15
  13.1 84.7 %copy-start.7 = (f32[2]{0:T(128)S(1)}, f32[2]{0:T(128)}, u32[]{:S(2)}) copy-start(f32[2]{0:T(128)} %param.22) | copy-start | bytes 28
  97.8 6.3 %copy-start.3 = (bf16[256,2048]{1,0:T(8,128)(2,1)S(1)}, bf16[256,2048]{1,0:T(8,128)(2,1)}, u32[]{:S(2)}) copy-start(bf16[256,2048]{1,0:T(8,128)(2,1)} %param.23) | copy-start | bytes 3145732
  104.1 5.2 %copy-start.4 = (f32[2,2048]{1,0:T(2,128)S(1)}, f32[2,2048]{1,0:T(2,128)}, u32[]{:S(2)}) copy-start(f32[2,2048]{1,0:T(2,128)} %param.25) | copy-start | bytes 49156
  104.1 14.3 %copy-start.2 = (bf16[32,2048]{1,0:T(8,128)(2,1)S(1)}, bf16[32,2048]{1,0:T(8,128)(2,1)}, u32[]{:S(2)}) copy-start(bf16[32,2048]{1,0:T(8,128)(2,1)} %param.18) | copy-start | bytes 393220
  105.2 13.0 %all-to-all-start = ((bf16[4,32,2048]{2,1,0:T(8,128)(2,1)}), bf16[4,32,2048]{2,1,0:T(8,128)(2,1)S(1)}, u32[]{:S(2)}, u32[]{:S(2)}) async-start(bf16[4,32,2048]{2,1,0:T(8,128)(2,1)} %bitcast.4), calls=%async_computation | async-start | bytes 1048576 | tf_op jit(solution)/shard_map/all_to_all | solution.py:30
  267.0 13.2 %all-to-all-start.5 = ((bf16[4,32,2048]{2,1,0:T(8,128)(2,1)}), bf16[4,32,2048]{2,1,0:T(8,128)(2,1)}, u32[]{:S(2)}, u32[]{:S(2)}) async-start(bf16[4,32,2048]{2,1,0:T(8,128)(2,1)} %broadcast_in_dim.81), calls=%async_computation.5 | async-start | bytes 1048576 | tf_op jit(solution)/shard_map/all_to_all | solution.py:36
  271.3 1.6 copy-start.6
  271.5 1.4 copy-start.1
  280.2 28.7 %all-to-all-start.3 = ((bf16[4,64,1,2,2048]{4,1,3,2,0:T(8,128)(2,1)}), bf16[4,64,1,2,2048]{4,1,3,2,0:T(8,128)(2,1)S(1)}, u32[]{:S(2)}, u32[]{:S(2)}) async-start(bf16[4,64,1,2,2048]{4,1,3,2,0:T(8,128)(2,1)} %copy.45), calls=%async_computation.3 | async-start | bytes 4194304 | tf_op jit(solution)/shard_map/all_to_all | solution.py:30
  308.8 11.1 %all-to-all-start.6 = ((bf16[4,32,2048]{2,1,0:T(8,128)(2,1)}), bf16[4,32,2048]{2,1,0:T(8,128)(2,1)}, u32[]{:S(2)}, u32[]{:S(2)}) async-start(bf16[4,32,2048]{2,1,0:T(8,128)(2,1)} %bitcast.146), calls=%async_computation.6 | async-start | bytes 1048576 | tf_op jit(solution)/shard_map/all_to_all | solution.py:30
  313.0 15.8 %copy-start.5 = (f32[32,2]{0,1:T(2,128)S(1)}, f32[32,2]{0,1:T(2,128)}, u32[]{:S(2)}) copy-start(f32[32,2]{0,1:T(2,128)} %param.27) | copy-start | bytes 772
  320.0 26.5 %all-to-all-start.4 = ((bf16[64,1,2,2048]{3,2,1,0:T(2,128)(2,1)}), bf16[64,1,2,2048]{3,2,1,0:T(2,128)(2,1)S(1)}, u32[]{:S(2)}, u32[]{:S(2)}) async-start(bf16[64,1,2,2048]{3,2,1,0:T(2,128)(2,1)} %copy.47), calls=%async_computation.4 | async-start | bytes 1048576 | tf_op jit(solution)/shard_map/all_to_all | solution.py:179
Sparse Core Ops, SparseCore 0:
  10.1 83.1 all-gather.1
where the time goes:
time: 358 us; the launch traced here: 356 us
  blocking collectives  145 us (41%)
  waiting for transfers between devices  129 us (36%)
  starting transfers between devices  25.3 us (7%)
  local copies, waits for them, and re-layouts  17.8 us (5%)
  matrix products  14.6 us (4%)
  between operations  13.7 us (4%)
  other arithmetic  11.5 us (3%)
    all_to_all x1, blocking collectives, per_device(): lax.all_to_all(outgoing, 'sp', split_axis=0, concat_axis=0, tiled=True)  117 us
    all_gather x1, waiting for transfers between devices, in_one_piece(): whole, at, done = (lax.all_gather(both, axis, axis=dim, tiled=True), 0, [])  80.2 us
    all_to_all x3, waiting for transfers between devices, summed_on_arrival(): blocks = lax.all_to_all(split_up(array, dim, peers), axis, 0, 0, tiled=True)  31.9 us
    all_to_all x1, blocking collectives, sent_to_all(): lax.all_to_all(jnp.broadcast_to(array[None], (peers, *array.shape)), axis...  28.5 us
    all_to_all x1, waiting for transfers between devices, per_device(): lax.all_to_all(expert_sum.astype(jnp.bfloat16), 'sp', split_axis=0, conca...  16.5 us
    all_to_all x3, starting transfers between devices, summed_on_arrival(): blocks = lax.all_to_all(split_up(array, dim, peers), axis, 0, 0, tiled=True)  12.2 us
    all_to_all x1, starting transfers between devices, per_device(): lax.all_to_all(expert_sum.astype(jnp.bfloat16), 'sp', split_axis=0, conca...  8.81 us
  transfers between devices with their start and end apart: 6, of which 5 were waited for; matrix products, arithmetic and copies ran while one was open for 6% of the time, Pallas kernels for 0%

commit v1 on v0

--- a/solution.py
+++ b/solution.py
@@ -1,11 +1,13 @@
+import functools
+
 import jax
 import jax.numpy as jnp
 from jax import lax
+from jax.experimental import pallas as pl
+from jax.experimental.pallas import tpu as pltpu
 from jax.sharding import PartitionSpec as P
 
-DH = 128
-
-
+LOG2E = 1.4426950408889634
 ALPHA = 8.0**0.25
 LN_EPS = 1e-05
 
@@ -55,35 +57,72 @@
     return (center * lax.rsqrt(spread + LN_EPS) * gain + shift).astype(jnp.bfloat16)
 
 
-def stick_terms(queries, keys_block, key_start, query_pos, offset, shard_len):
-    kv_local, group_size = offset.shape
-    query_count = queries.shape[0]
-    key_count = keys_block.shape[0]
-    head_dim = keys_block.shape[-1]
-    scores = jnp.einsum("tkgd,skd->kgts", queries, keys_block, preferred_element_type=jnp.float32)
-    scores = scores * head_dim ** (-0.5) + offset[:, :, None, None]
-    key_pos = key_start + jnp.arange(key_count, dtype=jnp.int32)
-    causal = key_pos[None, :] < query_pos[:, None]
-    leftover = jnp.where(causal, jax.nn.log_sigmoid(-scores), 0.0)
-    shape_five = (kv_local, group_size, query_count, key_count // shard_len, shard_len)
-    causal = causal.reshape(query_count, key_count // shard_len, shard_len)
-    return (scores.reshape(shape_five), causal, leftover.reshape(shape_five))
-
-
-def stick_block(queries, keys_block, values_block, key_start, query_pos, offset, shard_len, beyond):
-    scores, causal, leftover = stick_terms(
-        queries, keys_block, key_start, query_pos, offset, shard_len
-    )
-    within = lax.cumsum(leftover, axis=4, reverse=True) - leftover
-    totals = jnp.sum(leftover, axis=4)
-    beyond = beyond + lax.cumsum(totals, axis=3, reverse=True) - totals
-    exponent = jax.nn.log_sigmoid(scores) + within + beyond[..., None]
-    weights = jnp.where(causal[None, None], jnp.exp(exponent), 0.0).astype(jnp.bfloat16)
-    weights = weights.reshape(scores.shape[0], scores.shape[1], scores.shape[2], -1)
-    partial_out = jnp.einsum(
-        "kgts,skd->tkgd", weights, values_block, preferred_element_type=jnp.float32
-    )
-    return (partial_out, totals)
+def attend_kernel(chunk, sub, off_ref, q_ref, k_ref, v_ref, out_ref, acc):
+    me = lax.axis_index("sp")
+    rows = q_ref.shape[0]
+    heads = off_ref.shape[0]
+    dh = k_ref.shape[1]
+    scale2 = dh ** -0.5 * LOG2E
+    r = lax.broadcasted_iota(jnp.int32, (sub, sub), 0)
+    c = lax.broadcasted_iota(jnp.int32, (sub, sub), 1)
+    tri = jnp.where(r > c, 1.0, 0.0).astype(jnp.bfloat16)
+    last = (me * rows) // chunk
+    tpos = me * rows + lax.broadcasted_iota(jnp.int32, (rows, sub), 0)
+
+    def chunk_at(at, carries, masked, first):
+        jobs = []
+        for j in reversed(range(chunk // sub)):
+            base = pl.multiple_of(at * chunk + j * sub, sub)
+            k = k_ref[pl.ds(base, sub), :]
+            v = v_ref[pl.ds(base, sub), :]
+            mask = None
+            if masked:
+                mask = base + lax.broadcasted_iota(jnp.int32, (rows, sub), 1) < tpos
+            for h in range(heads):
+                q = q_ref[:, h * dh:(h + 1) * dh]
+                s = lax.dot_general(q, k, (((1,), (1,)), ((), ())), preferred_element_type=jnp.float32)
+                jobs.append((h, s, v, mask))
+        stage = []
+        for h, s, v, mask in jobs:
+            s = s * scale2 + off_ref[h] * LOG2E
+            sp = jnp.maximum(s, 0.0) + jnp.log2(1.0 + jnp.exp2(-jnp.abs(s)))
+            own = s - sp
+            if mask is not None:
+                sp = jnp.where(mask, sp, 0.0)
+            hi = sp.astype(jnp.bfloat16)
+            lo = (sp - hi.astype(jnp.float32)).astype(jnp.bfloat16)
+            after = jnp.dot(hi, tri, preferred_element_type=jnp.float32) + jnp.dot(lo, tri, preferred_element_type=jnp.float32)
+            stage.append((h, own - after, after[:, :1] + sp[:, :1], v, mask))
+        carries = list(carries)
+        parts = [None] * heads
+        for h, e, tot, v, mask in stage:
+            w = jnp.exp2(e - carries[h])
+            if mask is not None:
+                w = jnp.where(mask, w, 0.0)
+            p = jnp.dot(w.astype(jnp.bfloat16), v, preferred_element_type=jnp.float32)
+            parts[h] = p if parts[h] is None else parts[h] + p
+            carries[h] = carries[h] + tot
+        for h in range(heads):
+            sl = slice(h * dh, (h + 1) * dh)
+            acc[:, sl] = parts[h] if first else acc[:, sl] + parts[h]
+        return tuple(carries)
+
+    carries = chunk_at(last, tuple(jnp.zeros((rows, 1), jnp.float32) for _ in range(heads)), True, True)
+    lax.fori_loop(0, last, lambda n, cr: chunk_at(last - 1 - n, cr, False, False), carries)
+    out_ref[...] = acc[...].astype(jnp.bfloat16)
+
+
+def attend(offset, queries, keys, values):
+    rows, width = queries.shape
+    vmem = pl.BlockSpec(memory_space=pltpu.VMEM)
+    return pl.pallas_call(
+        functools.partial(attend_kernel, 1024, 256),
+        out_shape=jax.ShapeDtypeStruct((rows, width), jnp.bfloat16),
+        in_specs=[pl.BlockSpec(memory_space=pltpu.SMEM), vmem, vmem, vmem],
+        out_specs=vmem,
+        scratch_shapes=[pltpu.VMEM((rows, width), jnp.float32)],
+        name="attend",
+    )(offset, queries, keys, values)
 
 
 def per_device(
@@ -104,37 +143,9 @@
     w_shared_up,
     w_shared_down,
 ):
-    shard_len = query_rows.shape[0]
-    kv_local = key_rows.shape[1] // DH
-    heads_local = query_rows.shape[1] // DH
-    group_size = heads_local // kv_local
     sp_count = lax.axis_size("sp")
-    sp_index = lax.axis_index("sp")
-    queries = query_rows.reshape(shard_len, kv_local, group_size, DH)
-    offset = head_offset.reshape(kv_local, group_size)
-    query_pos = sp_index * shard_len + jnp.arange(shard_len, dtype=jnp.int32)
-    empty_out = jnp.zeros((shard_len, kv_local, group_size, DH), jnp.float32)
     all_keys, all_values = in_one_piece((key_rows, value_rows), "sp", 0, 1)
-    all_keys = all_keys.reshape(-1, kv_local, DH)
-    all_values = all_values.reshape(-1, kv_local, DH)
-    turn_count = min(16, sp_count)
-    block_len = shard_len * sp_count // turn_count
-    own_block = sp_index * shard_len // block_len
-
-    def turn(step_index, state_now):
-        total_out, passed = state_now
-        first_key = (own_block - step_index) * block_len
-        keys_block = lax.dynamic_slice_in_dim(all_keys, first_key, block_len, 0)
-        values_block = lax.dynamic_slice_in_dim(all_values, first_key, block_len, 0)
-        beyond = jnp.broadcast_to(passed[..., None], passed.shape + (block_len // shard_len,))
-        partial_out, totals = stick_block(
-            queries, keys_block, values_block, first_key, query_pos, offset, shard_len, beyond
-        )
-        return (total_out + partial_out, passed + jnp.sum(totals, axis=3))
-
-    start_state = (empty_out, jnp.zeros((kv_local, group_size, shard_len), jnp.float32))
-    attended, _ = lax.fori_loop(0, own_block + 1, turn, start_state)
-    attended = attended.astype(jnp.bfloat16).reshape(shard_len, heads_local * DH)
+    attended = attend(head_offset, query_rows, all_keys, all_values)
     rows_local = residual.shape[0]
     mixed = summed_on_arrival(
         jnp.dot(attended, w_out, preferred_element_type=jnp.float32).astype(jnp.bfloat16), "tp", 0

time: 358 us -> 271 us (0.76)
  blocking collectives: 145 us -> 59.5 us
  Pallas kernels: 0 us -> 4.1 us
    all_to_all x1, blocking collectives: 117 us -> 31 us  [per_device(): lax.all_to_all(outgoing, 'sp', split_axis=0, concat_axis=0, tiled=True)]
    reshape x1 -> x0, local copies, waits for them, and re-layouts: 4.46 us -> none  [per_device(): all_keys = all_keys.reshape(-1, kv_local, DH)]
    slice x0 -> x1, local copies, waits for them, and re-layouts: none -> 4.46 us  [in_one_piece(): done.append(lax.slice_in_dim(whole, at, at + a.shape[along], axis=along))]
    pallas_call x0 -> x1, Pallas kernels: none -> 4.1 us  [attend(): pl.pallas_call(functools.partial(attend_kernel, 1024, 256), out_shape=jax...]
  transfers between devices with their start and end apart: 6 -> 6, of which waited for: 5 -> 5; matrix products, arithmetic and copies ran while one was open for 6% -> 8% of each run, Pallas kernels for 0% -> 0%
where the time goes in v1:
time: 271 us; the launch traced here: 270 us
  waiting for transfers between devices  130 us (48%)
  blocking collectives  59.5 us (22%)
  starting transfers between devices  25.5 us (9%)
  local copies, waits for them, and re-layouts  16.6 us (6%)
  between operations  13.6 us (5%)
  matrix products  12.8 us (5%)
  other arithmetic  8.02 us (3%)
  Pallas kernels  4.1 us (2%)
    all_gather x1, waiting for transfers between devices, in_one_piece(): whole, at, done = (lax.all_gather(both, axis, axis=dim, tiled=True), 0, [])  81.3 us
    all_to_all x3, waiting for transfers between devices, summed_on_arrival(): blocks = lax.all_to_all(split_up(array, dim, peers), axis, 0, 0, tiled=True)  31.9 us
    all_to_all x1, blocking collectives, per_device(): lax.all_to_all(outgoing, 'sp', split_axis=0, concat_axis=0, tiled=True)  31 us
    all_to_all x1, blocking collectives, sent_to_all(): lax.all_to_all(jnp.broadcast_to(array[None], (peers, *array.shape)), axis...  28.5 us
    all_to_all x1, waiting for transfers between devices, per_device(): lax.all_to_all(expert_sum.astype(jnp.bfloat16), 'sp', split_axis=0, conca...  16.5 us
    all_to_all x3, starting transfers between devices, summed_on_arrival(): blocks = lax.all_to_all(split_up(array, dim, peers), axis, 0, 0, tiled=True)  12.3 us
    all_to_all x1, starting transfers between devices, per_device(): lax.all_to_all(expert_sum.astype(jnp.bfloat16), 'sp', split_axis=0, conca...  8.99 us
  transfers between devices with their start and end apart: 6, of which 5 were waited for; matrix products, arithmetic and copies ran while one was open for 8% of the time, Pallas kernels for 0%

profile of v1, /device:TPU:1, one launch (start us, length us, event | category | flops | bytes accessed | tf_op | source)
XLA Modules:
  0.0 269.8 jit_solution(5242478128078631379)
XLA Ops:
  6.5 1.5 pad_maximum_fusion
  12.0 81.3 %all-gather.2.cloned.1.call-done = bf16[8192,256]{1,0:T(8,128)(2,1)} async-done(((bf16[128,256]{1,0:T(8,128)(2,1)}), bf16[8192,256]{1,0:T(8,128)(2,1)}) %all-gather.2.cloned.1.call-update) | async-done | bytes 4194320 | tf_op jit(solution)/shard_map/all_gather | solution.py:17
  93.3 4.5 %fusion.28 = (bf16[8192,128]{1,0:T(8,128)(2,1)}, bf16[8192,128]{1,0:T(8,128)(2,1)}) fusion(bf16[8192,256]{1,0:T(8,128)(2,1)} %all-gather.2.cloned.1.call-done), kind=kLoop, calls=%fused_computation.63 | loop fusion | bytes 8388608 | tf_op jit(solution)/shard_map/slice | solution.py:19
  97.8 4.1 %attend.1 = bf16[128,256]{1,0:T(8,128)(2,1)} custom-call(f32[2]{0:T(128)} %off_ref.1, bf16[128,256]{1,0:T(8,128)(2,1)} %q_ref.1, bf16[8192,128]{1,0:T(8,128)(2,1)} %get-tuple-element.6.k_ref, bf16[8192,128]{1,0:T(8,128)(2,1)} %get-tuple-element.5.v_ref), custom_call_target="tpu_custom_call" | custom-call | tf_op jit(solution)/shard_map/attend/pallas_call | solution.py:118
  101.9 2.0 convolution_convert_fusion.2
  103.9 4.0 %all-to-all-start = ((bf16[4,32,2048]{2,1,0:T(8,128)(2,1)}), bf16[4,32,2048]{2,1,0:T(8,128)(2,1)S(1)}, u32[]{:S(2)}, u32[]{:S(2)}) async-start(bf16[4,32,2048]{2,1,0:T(8,128)(2,1)} %bitcast), calls=%async_computation | async-start | bytes 1048576 | tf_op jit(solution)/shard_map/all_to_all | solution.py:32
  107.9 9.0 %all-to-all-done = bf16[4,32,2048]{2,1,0:T(8,128)(2,1)S(1)} async-done(((bf16[4,32,2048]{2,1,0:T(8,128)(2,1)}), bf16[4,32,2048]{2,1,0:T(8,128)(2,1)S(1)}, u32[]{:S(2)}, u32[]{:S(2)}) %all-to-all-start) | async-done | bytes 524320 | tf_op jit(solution)/shard_map/all_to_all | solution.py:32
  119.3 31.0 %all_to_all.35 = bf16[64,1,2,2048]{3,2,1,0:T(2,128)(2,1)S(1)} all-to-all(bf16[64,1,2,2048]{3,2,1,0:T(2,128)(2,1)S(1)} %broadcast_select_fusion), channel_id=1, replica_groups=mesh['sp'=64,'tp'=4] {'sp'}, dimensions={0} | all-to-all | bytes 1048576 | tf_op jit(solution)/shard_map/all_to_all | solution.py:170
  150.7 28.5 %all_to_all.36 = bf16[4,64,1,2,2048]{4,1,3,2,0:T(8,128)(2,1)S(1)} all-to-all(bf16[4,64,1,2,2048]{4,1,3,2,0:T(8,128)(2,1)S(1)} %broadcast_in_dim.45), channel_id=1, replica_groups=mesh['sp'=64,'tp'=4] {'tp'}, dimensions={0} | all-to-all | bytes 4194304 | tf_op jit(solution)/shard_map/all_to_all | solution.py:38
  180.1 4.1 %all-to-all-start.5 = ((bf16[4,32,2048]{2,1,0:T(8,128)(2,1)}), bf16[4,32,2048]{2,1,0:T(8,128)(2,1)}, u32[]{:S(2)}, u32[]{:S(2)}) async-start(bf16[4,32,2048]{2,1,0:T(8,128)(2,1)} %broadcast_in_dim.46), calls=%async_computation.5 | async-start | bytes 1048576 | tf_op jit(solution)/shard_map/all_to_all | solution.py:38
  184.4 1.3 copy-done.1
  185.8 1.5 convolution_bitcast_fusion.1
  187.3 4.3 %convolution_convert_fusion = bf16[256,2,2048]{2,0,1:T(8,128)(2,1)S(1)} fusion(bf16[256,2,2048]{2,0,1:T(8,128)(2,1)} %bitcast.73, bf16[1,256,2048]{2,1,0:T(8,128)(2,1)S(1)} %copy-done, bf16[1,2048,256]{2,1,0:T(8,128)(2,1)} %param.27, f32[256,1,2,256]{3,0,2,1:T(8,128)} %convolution_bitcast_fusion.1), kind=kOutput, calls=%fused_computation.3 | convolution fusion | flops 1075576832 | bytes 6815744 | tf_op jit(solution)/shard_map/aecf,efd->aecd/dot_general | solution.py:179
  191.6 1.5 copy.30
  193.1 4.2 %all-to-all-start.3 = ((bf16[4,64,1,2,2048]{4,1,3,2,0:T(8,128)(2,1)}), bf16[4,64,1,2,2048]{4,1,3,2,0:T(8,128)(2,1)S(1)}, u32[]{:S(2)}, u32[]{:S(2)}) async-start(bf16[4,64,1,2,2048]{4,1,3,2,0:T(8,128)(2,1)} %copy.30), calls=%async_computation.3 | async-start | bytes 4194304 | tf_op jit(solution)/shard_map/all_to_all | solution.py:32
  197.3 1.7 fusion.31
  199.0 3.3 %convolution_convert_fusion.1 = bf16[128,2048]{1,0:T(8,128)(2,1)} fusion(bf16[256,2048]{1,0:T(8,128)(2,1)} %param.31, bf16[128,2048]{1,0:T(8,128)(2,1)} %bitcast.28, bf16[2048,256]{1,0:T(8,128)(2,1)} %param.30, f32[128,256]{1,0:T(8,128)S(1)} %fusion.31), kind=kOutput, calls=%fused_computation.4 | convolution fusion | flops 268894208 | bytes 3276800 | tf_op jit(solution)/shard_map/dot_general | solution.py:185
  202.3 19.6 %all-to-all-done.3 = bf16[4,64,1,2,2048]{4,1,3,2,0:T(8,128)(2,1)S(1)} async-done(((bf16[4,64,1,2,2048]{4,1,3,2,0:T(8,128)(2,1)}), bf16[4,64,1,2,2048]{4,1,3,2,0:T(8,128)(2,1)S(1)}, u32[]{:S(2)}, u32[]{:S(2)}) %all-to-all-start.3) | async-done | bytes 2097184 | tf_op jit(solution)/shard_map/all_to_all | solution.py:32
  221.9 4.1 %all-to-all-start.6 = ((bf16[4,32,2048]{2,1,0:T(8,128)(2,1)}), bf16[4,32,2048]{2,1,0:T(8,128)(2,1)}, u32[]{:S(2)}, u32[]{:S(2)}) async-start(bf16[4,32,2048]{2,1,0:T(8,128)(2,1)} %bitcast.71), calls=%async_computation.6 | async-start | bytes 1048576 | tf_op jit(solution)/shard_map/all_to_all | solution.py:32
  226.1 1.3 reduce_sum.96
  227.4 2.4 copy.32
  229.8 3.3 %all-to-all-done.6 = bf16[4,32,2048]{2,1,0:T(8,128)(2,1)} async-done(((bf16[4,32,2048]{2,1,0:T(8,128)(2,1)}), bf16[4,32,2048]{2,1,0:T(8,128)(2,1)}, u32[]{:S(2)}, u32[]{:S(2)}) %all-to-all-start.6) | async-done | bytes 524320 | tf_op jit(solution)/shard_map/all_to_all | solution.py:32
  233.0 9.0 %all-to-all-start.4 = ((bf16[64,1,2,2048]{3,2,1,0:T(2,128)(2,1)}), bf16[64,1,2,2048]{3,2,1,0:T(2,128)(2,1)S(1)}, u32[]{:S(2)}, u32[]{:S(2)}) async-start(bf16[64,1,2,2048]{3,2,1,0:T(2,128)(2,1)} %copy.32), calls=%async_computation.4 | async-start | bytes 1048576 | tf_op jit(solution)/shard_map/all_to_all | solution.py:190
  243.3 16.5 %all-to-all-done.4 = bf16[64,1,2,2048]{3,2,1,0:T(2,128)(2,1)S(1)} async-done(((bf16[64,1,2,2048]{3,2,1,0:T(2,128)(2,1)}), bf16[64,1,2,2048]{3,2,1,0:T(2,128)(2,1)S(1)}, u32[]{:S(2)}, u32[]{:S(2)}) %all-to-all-start.4) | async-done | bytes 524320 | tf_op jit(solution)/shard_map/all_to_all | solution.py:190
  (58 shorter events, 12.2 us)
Async XLA Ops:
  6.5 180.8 %copy-start = (bf16[1,256,2048]{2,1,0:T(8,128)(2,1)S(1)}, bf16[1,256,2048]{2,1,0:T(8,128)(2,1)}, u32[]{:S(2)}) copy-start(bf16[1,256,2048]{2,1,0:T(8,128)(2,1)} %param.28) | copy-start | bytes 3145732
  6.5 86.8 %all-gather.2.cloned.1.call-start = ((), (), s32[]{:S(2)}) async-start(), calls=%async_computation.7 | async-start | bytes 4259840 | tf_op jit(solution)/shard_map/all_gather | solution.py:17
  97.8 4.1 %copy-start.3 = (bf16[256,2048]{1,0:T(8,128)(2,1)S(1)}, bf16[256,2048]{1,0:T(8,128)(2,1)}, u32[]{:S(2)}) copy-start(bf16[256,2048]{1,0:T(8,128)(2,1)} %param.21) | copy-start | bytes 3145732
  101.9 6.0 %copy-start.4 = (f32[2,2048]{1,0:T(2,128)S(1)}, f32[2,2048]{1,0:T(2,128)}, u32[]{:S(2)}) copy-start(f32[2,2048]{1,0:T(2,128)} %param.23) | copy-start | bytes 49156
  101.9 15.1 %copy-start.2 = (bf16[32,2048]{1,0:T(8,128)(2,1)S(1)}, bf16[32,2048]{1,0:T(8,128)(2,1)}, u32[]{:S(2)}) copy-start(bf16[32,2048]{1,0:T(8,128)(2,1)} %param.16) | copy-start | bytes 393220
  103.9 13.0 %all-to-all-start = ((bf16[4,32,2048]{2,1,0:T(8,128)(2,1)}), bf16[4,32,2048]{2,1,0:T(8,128)(2,1)S(1)}, u32[]{:S(2)}, u32[]{:S(2)}) async-start(bf16[4,32,2048]{2,1,0:T(8,128)(2,1)} %bitcast), calls=%async_computation | async-start | bytes 1048576 | tf_op jit(solution)/shard_map/all_to_all | solution.py:32
  180.1 13.0 %all-to-all-start.5 = ((bf16[4,32,2048]{2,1,0:T(8,128)(2,1)}), bf16[4,32,2048]{2,1,0:T(8,128)(2,1)}, u32[]{:S(2)}, u32[]{:S(2)}) async-start(bf16[4,32,2048]{2,1,0:T(8,128)(2,1)} %broadcast_in_dim.46), calls=%async_computation.5 | async-start | bytes 1048576 | tf_op jit(solution)/shard_map/all_to_all | solution.py:38
  184.2 1.6 copy-start.6
  184.4 1.4 copy-start.1
  193.1 28.8 %all-to-all-start.3 = ((bf16[4,64,1,2,2048]{4,1,3,2,0:T(8,128)(2,1)}), bf16[4,64,1,2,2048]{4,1,3,2,0:T(8,128)(2,1)S(1)}, u32[]{:S(2)}, u32[]{:S(2)}) async-start(bf16[4,64,1,2,2048]{4,1,3,2,0:T(8,128)(2,1)} %copy.30), calls=%async_computation.3 | async-start | bytes 4194304 | tf_op jit(solution)/shard_map/all_to_all | solution.py:32
  221.9 11.1 %all-to-all-start.6 = ((bf16[4,32,2048]{2,1,0:T(8,128)(2,1)}), bf16[4,32,2048]{2,1,0:T(8,128)(2,1)}, u32[]{:S(2)}, u32[]{:S(2)}) async-start(bf16[4,32,2048]{2,1,0:T(8,128)(2,1)} %bitcast.71), calls=%async_computation.6 | async-start | bytes 1048576 | tf_op jit(solution)/shard_map/all_to_all | solution.py:32
  226.0 16.0 %copy-start.5 = (f32[32,2]{0,1:T(2,128)S(1)}, f32[32,2]{0,1:T(2,128)}, u32[]{:S(2)}) copy-start(f32[32,2]{0,1:T(2,128)} %param.25) | copy-start | bytes 772
  233.0 26.7 %all-to-all-start.4 = ((bf16[64,1,2,2048]{3,2,1,0:T(2,128)(2,1)}), bf16[64,1,2,2048]{3,2,1,0:T(2,128)(2,1)S(1)}, u32[]{:S(2)}, u32[]{:S(2)}) async-start(bf16[64,1,2,2048]{3,2,1,0:T(2,128)(2,1)} %copy.32), calls=%async_computation.4 | async-start | bytes 1048576 | tf_op jit(solution)/shard_map/all_to_all | solution.py:190
Sparse Core Ops, SparseCore 0:
  10.1 83.1 all-gather.1

commit v2 on v1

--- a/solution.py
+++ b/solution.py
@@ -12,15 +12,6 @@
 LN_EPS = 1e-05
 
 
-def in_one_piece(arrays, axis, dim, along):
-    both = jnp.concatenate(arrays, axis=along)
-    whole, at, done = (lax.all_gather(both, axis, axis=dim, tiled=True), 0, [])
-    for a in arrays:
-        done.append(lax.slice_in_dim(whole, at, at + a.shape[along], axis=along))
-        at += a.shape[along]
-    return tuple(done)
-
-
 def split_up(array, dim, peers):
     dims = array.shape
     blocks = array.reshape(*dims[:dim], peers, dims[dim] // peers, *dims[dim + 1 :])
@@ -57,70 +48,275 @@
     return (center * lax.rsqrt(spread + LN_EPS) * gain + shift).astype(jnp.bfloat16)
 
 
-def attend_kernel(chunk, sub, off_ref, q_ref, k_ref, v_ref, out_ref, acc):
+def cross(sp_count):
+    rows_x = 4
+    return sp_count // (2 * rows_x), rows_x
+
+
+def attend_kernel(rows_z, rows_x, off_ref, q_ref, k_ref, v_ref, out_ref,
+                  keys, values, right, left, carry, send, recv, local):
     me = lax.axis_index("sp")
+    z, x, c = (
+        lax.div(me, 2 * rows_x),
+        lax.rem(lax.div(me, 2), rows_x),
+        lax.rem(me, 2),
+    )
     rows = q_ref.shape[0]
     heads = off_ref.shape[0]
     dh = k_ref.shape[1]
-    scale2 = dh ** -0.5 * LOG2E
-    r = lax.broadcasted_iota(jnp.int32, (sub, sub), 0)
-    c = lax.broadcasted_iota(jnp.int32, (sub, sub), 1)
-    tri = jnp.where(r > c, 1.0, 0.0).astype(jnp.bfloat16)
-    last = (me * rows) // chunk
-    tpos = me * rows + lax.broadcasted_iota(jnp.int32, (rows, sub), 0)
-
-    def chunk_at(at, carries, masked, first):
-        jobs = []
-        for j in reversed(range(chunk // sub)):
-            base = pl.multiple_of(at * chunk + j * sub, sub)
-            k = k_ref[pl.ds(base, sub), :]
-            v = v_ref[pl.ds(base, sub), :]
+    half = rows // 2
+    reach = rows_z // 2
+
+    def at(zz, xx, cc):
+        return (zz * rows_x + xx) * 2 + cc
+
+    def turn(value, by, size):
+        return lax.rem(value + (by + size), size)
+
+    z_up, z_down = turn(z, 1, rows_z), turn(z, -1, rows_z)
+    x_up, x_down = turn(x, 1, rows_x), turn(x, -1, rows_x)
+    x_far = turn(x, 2, rows_x)
+    to_z = {1: at(z_up, x, c), -1: at(z_down, x, c)}
+    to_x = {1: at(z, x_up, c), -1: at(z, x_down, c)}
+    partner = at(z, x, 1 - c)
+
+    names = {}
+
+    def copy(name, src, dst, target):
+        slot = names.setdefault(name, len(names))
+        return pltpu.make_async_remote_copy(
+            src_ref=src, dst_ref=dst, send_sem=send.at[slot], recv_sem=recv.at[slot],
+            device_id={"sp": target}, device_id_type=pl.DeviceIdType.MESH,
+        )
+
+    started = []
+
+    def begin(*args):
+        job = copy(*args)
+        job.start()
+        started.append(job)
+
+    def arrive(name, dst):
+        copy(name, dst, dst, partner).wait_recv()
+
+    barrier = pltpu.get_barrier_semaphore()
+    peers = (to_z[1], to_z[-1], to_x[1], to_x[-1], partner)
+    for peer in peers:
+        pl.semaphore_signal(barrier, inc=1, device_id={"sp": peer}, device_id_type=pl.DeviceIdType.MESH)
+    pl.semaphore_wait(barrier, len(peers))
+
+    keep_k = pltpu.make_async_copy(k_ref, keys.at[z, x, c], local.at[0])
+    keep_v = pltpu.make_async_copy(v_ref, values.at[z, x, c], local.at[1])
+    keep_k.start()
+    keep_v.start()
+    own_k, own_v = keys.at[z, x, c], values.at[z, x, c]
+    for way in (1, -1):
+        begin(("kx", way), k_ref, own_k, to_x[way])
+    for way in (1, -1):
+        begin(("vz", way, 1), v_ref, own_v, to_z[way])
+    for way in (1, -1):
+        begin(("vx", 0, 0, way), v_ref, own_v, to_x[way])
+
+    lower, upper = pl.ds(0, half), pl.ds(half, half)
+    side = {1: x_down, -1: x_up}
+    part = {1: lower, -1: upper}
+
+    def across(tag, buf, zz):
+        for way in (1, -1):
+            arrive(tag + (way,), buf.at[zz, side[way], c])
+            piece = buf.at[zz, side[way], c, part[way]]
+            begin(tag + ("far", way), piece, piece, to_x[way])
+
+    def across_end(tag, buf, zz):
+        for way in (1, -1):
+            arrive(tag + ("far", way), buf.at[zz, x_far, c, part[way]])
+
+    def share(tag, buf, zz):
+        begin(tag + ("peer",), buf.at[zz, :, c], buf.at[zz, :, c], partner)
+
+    def shared(tag, buf, zz):
+        other = buf.at[zz, :, 1 - c]
+        arrive(tag + ("peer",), other)
+
+    pieces = {0: pl.ds(0, rows_x // 2), 1: pl.ds(rows_x // 2, rows_x // 2)}
+
+    def forward_k(way, zz, step):
+        for sub in (0, 1):
+            if step == reach and (sub == 0) != (way == 1):
+                continue
+            block = keys.at[zz, pieces[sub], c]
+            begin(("kz", way, step, sub), block, block, to_z[way])
+
+    across(("kx",), keys, z)
+    keep_k.wait()
+    keep_v.wait()
+    across_end(("kx",), keys, z)
+    for way in (1, -1):
+        forward_k(way, z, 1)
+    share(("k", 0, 0), keys, z)
+
+    def slab_of(way, step):
+        return turn(z, -way * step, rows_z)
+
+    def z_step_v(step):
+        for way in (1, -1):
+            zz = slab_of(way, step)
+            if step < reach:
+                block = values.at[zz, x, c]
+                arrive(("vz", way, step), block)
+                if step + 1 < reach:
+                    begin(("vz", way, step + 1), block, block, to_z[way])
+                else:
+                    piece = values.at[zz, x, c, part[way]]
+                    begin(("vz", way, step + 1), piece, piece, to_z[way])
+                for side_way in (1, -1):
+                    begin(("vx", way, step, side_way), block, block, to_x[side_way])
+            else:
+                piece = values.at[zz, x, c, part[way]]
+                arrive(("vz", way, step), piece)
+        if step == reach:
+            block = values.at[slab_of(1, step), x, c]
+            for side_way in (1, -1):
+                begin(("vx", 1, step, side_way), block, block, to_x[side_way])
+
+    def slabs_at(step):
+        if step == 0:
+            return ((0, 0),)
+        if step == reach:
+            return ((1, step),)
+        return ((1, step), (-1, step))
+
+    def z_step_k(step):
+        for way in (1, -1):
+            zz = slab_of(way, step)
+            for sub in (0, 1):
+                if step == reach and (sub == 0) != (way == 1):
+                    continue
+                arrive(("kz", way, step, sub), keys.at[zz, pieces[sub], c])
+            if step < reach:
+                forward_k(way, zz, step + 1)
+        for way, stp in slabs_at(step):
+            share(("k", way, stp), keys, slab_of(way, stp))
+
+    scale2 = dh**-0.5 * LOG2E
+    sub = 2 * rows
+    r_at = lax.broadcasted_iota(jnp.int32, (sub, sub), 0)
+    c_at = lax.broadcasted_iota(jnp.int32, (sub, sub), 1)
+    after_of = jnp.where(r_at > c_at, 1.0, 0.0).astype(jnp.bfloat16)
+    t_in_slab = (x * 2 + c) * rows + lax.broadcasted_iota(jnp.int32, (rows, sub), 0)
+
+    def slab(zz, carries, masked):
+        stage = []
+        for j in reversed(range(rows_x)):
+            k = keys[zz, j].reshape(sub, dh)
+            v = values[zz, j].reshape(sub, dh)
             mask = None
             if masked:
-                mask = base + lax.broadcasted_iota(jnp.int32, (rows, sub), 1) < tpos
+                mask = j * sub + lax.broadcasted_iota(jnp.int32, (rows, sub), 1) < t_in_slab
             for h in range(heads):
-                q = q_ref[:, h * dh:(h + 1) * dh]
+                q = q_ref[:, h * dh : (h + 1) * dh]
                 s = lax.dot_general(q, k, (((1,), (1,)), ((), ())), preferred_element_type=jnp.float32)
-                jobs.append((h, s, v, mask))
-        stage = []
-        for h, s, v, mask in jobs:
-            s = s * scale2 + off_ref[h] * LOG2E
-            sp = jnp.maximum(s, 0.0) + jnp.log2(1.0 + jnp.exp2(-jnp.abs(s)))
-            own = s - sp
-            if mask is not None:
-                sp = jnp.where(mask, sp, 0.0)
-            hi = sp.astype(jnp.bfloat16)
-            lo = (sp - hi.astype(jnp.float32)).astype(jnp.bfloat16)
-            after = jnp.dot(hi, tri, preferred_element_type=jnp.float32) + jnp.dot(lo, tri, preferred_element_type=jnp.float32)
-            stage.append((h, own - after, after[:, :1] + sp[:, :1], v, mask))
+                s = s * scale2 + off_ref[h] * LOG2E
+                sp = jnp.maximum(s, 0.0) + jnp.log2(1.0 + jnp.exp2(-jnp.abs(s)))
+                own = s - sp
+                if masked:
+                    sp = jnp.where(mask, sp, 0.0)
+                hi = sp.astype(jnp.bfloat16)
+                lo = (sp - hi.astype(jnp.float32)).astype(jnp.bfloat16)
+                after = jnp.dot(hi, after_of, preferred_element_type=jnp.float32)
+                after = after + jnp.dot(lo, after_of, preferred_element_type=jnp.float32)
+                stage.append((h, own - after, after[:, :1] + sp[:, :1], v, mask))
         carries = list(carries)
         parts = [None] * heads
-        for h, e, tot, v, mask in stage:
-            w = jnp.exp2(e - carries[h])
-            if mask is not None:
+        for h, exponent, total, v, mask in stage:
+            w = jnp.exp2(exponent - carries[h])
+            if masked:
                 w = jnp.where(mask, w, 0.0)
-            p = jnp.dot(w.astype(jnp.bfloat16), v, preferred_element_type=jnp.float32)
-            parts[h] = p if parts[h] is None else parts[h] + p
-            carries[h] = carries[h] + tot
+            piece = jnp.dot(w.astype(jnp.bfloat16), v, preferred_element_type=jnp.float32)
+            parts[h] = piece if parts[h] is None else parts[h] + piece
+            carries[h] = carries[h] + total
+        return parts, carries
+
+    def columns(h):
+        return slice(h * dh, (h + 1) * dh)
+
+    def put_carry(carries):
         for h in range(heads):
-            sl = slice(h * dh, (h + 1) * dh)
-            acc[:, sl] = parts[h] if first else acc[:, sl] + parts[h]
-        return tuple(carries)
-
-    carries = chunk_at(last, tuple(jnp.zeros((rows, 1), jnp.float32) for _ in range(heads)), True, True)
-    lax.fori_loop(0, last, lambda n, cr: chunk_at(last - 1 - n, cr, False, False), carries)
-    out_ref[...] = acc[...].astype(jnp.bfloat16)
+            carry[h] = jnp.broadcast_to(carries[h], (rows, dh))
+
+    def own_slab():
+        parts, carries = slab(z, [jnp.zeros((rows, 1), jnp.float32)] * heads, True)
+        for h in range(heads):
+            right[:, columns(h)] = parts[h]
+        put_carry(carries)
+        left[...] = jnp.zeros_like(left)
+
+    def right_slab(step):
+        @pl.when(z >= step)
+        def _():
+            parts, carries = slab(z - step, [carry[h][:, :1] for h in range(heads)], False)
+            for h in range(heads):
+                right[:, columns(h)] = right[:, columns(h)] + parts[h]
+            put_carry(carries)
+
+    def left_slab(step):
+        @pl.when(z + step >= rows_z)
+        def _():
+            parts, totals = slab(z + step - rows_z, [jnp.zeros((rows, 1), jnp.float32)] * heads, False)
+            for h in range(heads):
+                left[:, columns(h)] = parts[h] + jnp.exp2(-totals[h]) * left[:, columns(h)]
+
+    for step in range(reach + 1):
+        if step > 0:
+            z_step_k(step)
+        for way, stp in slabs_at(step):
+            across(("vx", way, stp), values, slab_of(way, stp))
+        if step < reach:
+            z_step_v(step + 1)
+        for way, stp in slabs_at(step):
+            across_end(("vx", way, stp), values, slab_of(way, stp))
+            share(("v", way, stp), values, slab_of(way, stp))
+        ready = step - 1 if step < reach else None
+        for done in ([step - 1] if step > 0 else []) + ([reach] if step == reach else []):
+            for way, stp in slabs_at(done):
+                shared(("k", way, stp), keys, slab_of(way, stp))
+                shared(("v", way, stp), values, slab_of(way, stp))
+            if done == 0:
+                own_slab()
+            else:
+                right_slab(done)
+                if done < reach:
+                    left_slab(done)
+    for h in range(heads):
+        cols = columns(h)
+        out_ref[:, cols] = (right[:, cols] + jnp.exp2(-carry[h]) * left[:, cols]).astype(jnp.bfloat16)
+    for job in started:
+        job.wait_send()
 
 
 def attend(offset, queries, keys, values):
     rows, width = queries.shape
+    dh = keys.shape[1]
+    heads = offset.shape[0]
+    rows_z, rows_x = cross(lax.axis_size("sp"))
     vmem = pl.BlockSpec(memory_space=pltpu.VMEM)
+    whole = pltpu.VMEM((rows_z, rows_x, 2, rows, dh), jnp.bfloat16)
     return pl.pallas_call(
-        functools.partial(attend_kernel, 1024, 256),
+        functools.partial(attend_kernel, rows_z, rows_x),
         out_shape=jax.ShapeDtypeStruct((rows, width), jnp.bfloat16),
         in_specs=[pl.BlockSpec(memory_space=pltpu.SMEM), vmem, vmem, vmem],
         out_specs=vmem,
-        scratch_shapes=[pltpu.VMEM((rows, width), jnp.float32)],
+        scratch_shapes=[
+            whole,
+            whole,
+            pltpu.VMEM((rows, width), jnp.float32),
+            pltpu.VMEM((rows, width), jnp.float32),
+            pltpu.VMEM((heads, rows, dh), jnp.float32),
+            pltpu.SemaphoreType.DMA((96,)),
+            pltpu.SemaphoreType.DMA((96,)),
+            pltpu.SemaphoreType.DMA((2,)),
+        ],
+        compiler_params=pltpu.CompilerParams(collective_id=0, has_side_effects=True),
         name="attend",
     )(offset, queries, keys, values)
 
@@ -144,8 +340,7 @@
     w_shared_down,
 ):
     sp_count = lax.axis_size("sp")
-    all_keys, all_values = in_one_piece((key_rows, value_rows), "sp", 0, 1)
-    attended = attend(head_offset, query_rows, all_keys, all_values)
+    attended = attend(head_offset, query_rows, key_rows, value_rows)
     rows_local = residual.shape[0]
     mixed = summed_on_arrival(
         jnp.dot(attended, w_out, preferred_element_type=jnp.float32).astype(jnp.bfloat16), "tp", 0

time: 271 us -> 203 us (0.75)
  waiting for transfers between devices: 130 us -> 46.6 us
  Pallas kernels: 4.1 us -> 44.7 us
  between operations: 13.6 us -> 0.27 us
  local copies, waits for them, and re-layouts: 16.6 us -> 10.9 us
  blocking collectives: 59.5 us -> 55.4 us
    all_gather x1 -> x0, waiting for transfers between devices: 81.3 us -> none  [in_one_piece(): whole, at, done = (lax.all_gather(both, axis, axis=dim, tiled=True), 0, [])]
    pallas_call x1, Pallas kernels: 4.1 us -> 44.7 us  [attend(): pl.pallas_call(functools.partial(attend_kernel, rows_z, rows_x), out_shap...]
    slice x1 -> x0, local copies, waits for them, and re-layouts: 4.46 us -> none  [in_one_piece(): done.append(lax.slice_in_dim(whole, at, at + a.shape[along], axis=along))]
    all_to_all x1, blocking collectives: 31 us -> 26.9 us  [per_device(): lax.all_to_all(outgoing, 'sp', split_axis=0, concat_axis=0, tiled=True)]
  transfers between devices with their start and end apart: 6 -> 5, of which waited for: 5 -> 4; matrix products, arithmetic and copies ran while one was open for 8% -> 10% of each run, Pallas kernels for 0% -> 0%
where the time goes in v2:
time: 203 us; the launch traced here: 202 us
  blocking collectives  55.4 us (27%)
  waiting for transfers between devices  46.6 us (23%)
  Pallas kernels  44.7 us (22%)
  starting transfers between devices  25.5 us (13%)
  matrix products  13.1 us (6%)
  local copies, waits for them, and re-layouts  10.9 us (5%)
  other arithmetic  5.84 us (3%)
    pallas_call x1, Pallas kernels, attend(): pl.pallas_call(functools.partial(attend_kernel, rows_z, rows_x), out_shap...  44.7 us
    all_to_all x3, waiting for transfers between devices, summed_on_arrival(): blocks = lax.all_to_all(split_up(array, dim, peers), axis, 0, 0, tiled=True)  30.2 us
    all_to_all x1, blocking collectives, sent_to_all(): lax.all_to_all(jnp.broadcast_to(array[None], (peers, *array.shape)), axis...  28.5 us
    all_to_all x1, blocking collectives, per_device(): lax.all_to_all(outgoing, 'sp', split_axis=0, concat_axis=0, tiled=True)  26.9 us
    all_to_all x1, waiting for transfers between devices, per_device(): lax.all_to_all(expert_sum.astype(jnp.bfloat16), 'sp', split_axis=0, conca...  16.5 us
    all_to_all x3, starting transfers between devices, summed_on_arrival(): blocks = lax.all_to_all(split_up(array, dim, peers), axis, 0, 0, tiled=True)  12.5 us
    all_to_all x1, starting transfers between devices, per_device(): lax.all_to_all(expert_sum.astype(jnp.bfloat16), 'sp', split_axis=0, conca...  8.81 us
    dot_general x1, matrix products, per_device(): jnp.einsum('aecf,efd->aecd', hidden, w_exp_down, preferred_element_type=j...  4.29 us
  transfers between devices with their start and end apart: 5, of which 4 were waited for; matrix products, arithmetic and copies ran while one was open for 10% of the time, Pallas kernels for 0%

profile of v2, /device:TPU:1, one launch (start us, length us, event | category | flops | bytes accessed | tf_op | source)
XLA Modules:
  0.0 202.3 jit_solution(12825220702131454281)
XLA Ops:
  0.0 44.7 %attend.1 = bf16[128,256]{1,0:T(8,128)(2,1)} custom-call(f32[2]{0:T(128)} %off_ref.1, bf16[128,256]{1,0:T(8,128)(2,1)} %q_ref.1, bf16[128,128]{1,0:T(8,128)(2,1)} %k_ref.1, bf16[128,128]{1,0:T(8,128)(2,1)} %v_ref.1), custom_call_target="tpu_custom_call" | custom-call | tf_op jit(solution)/shard_map/attend/pallas_call | solution.py:304
  44.7 2.4 %convolution_convert_fusion.2 = bf16[128,2048]{1,0:T(8,128)(2,1)} fusion(bf16[128,256]{1,0:T(8,128)(2,1)} %attend.1, bf16[256,2048]{1,0:T(8,128)(2,1)} %param.21), kind=kOutput, calls=%fused_computation.5 | convolution fusion | flops 134479872 | bytes 1638400 | tf_op jit(solution)/shard_map/dot_general | solution.py:346
  47.1 4.2 %all-to-all-start = ((bf16[4,32,2048]{2,1,0:T(8,128)(2,1)}), bf16[4,32,2048]{2,1,0:T(8,128)(2,1)S(1)}, u32[]{:S(2)}, u32[]{:S(2)}) async-start(bf16[4,32,2048]{2,1,0:T(8,128)(2,1)} %bitcast), calls=%async_computation | async-start | bytes 1048576 | tf_op jit(solution)/shard_map/all_to_all | solution.py:23
  52.0 1.0 scatter_custom_fusion
  53.3 7.3 %all-to-all-done = bf16[4,32,2048]{2,1,0:T(8,128)(2,1)S(1)} async-done(((bf16[4,32,2048]{2,1,0:T(8,128)(2,1)}), bf16[4,32,2048]{2,1,0:T(8,128)(2,1)S(1)}, u32[]{:S(2)}, u32[]{:S(2)}) %all-to-all-start) | async-done | bytes 524320 | tf_op jit(solution)/shard_map/all_to_all | solution.py:23
  61.2 0.9 gather_fusion
  63.0 26.9 %all_to_all.35 = bf16[64,1,2,2048]{3,2,1,0:T(2,128)(2,1)S(1)} all-to-all(bf16[64,1,2,2048]{3,2,1,0:T(2,128)(2,1)S(1)} %broadcast_select_fusion), channel_id=1, replica_groups=mesh['sp'=64,'tp'=4] {'sp'}, dimensions={0} | all-to-all | bytes 1048576 | tf_op jit(solution)/shard_map/all_to_all | solution.py:365
  90.3 28.5 %all_to_all.36 = bf16[4,64,1,2,2048]{4,1,3,2,0:T(8,128)(2,1)S(1)} all-to-all(bf16[4,64,1,2,2048]{4,1,3,2,0:T(8,128)(2,1)S(1)} %broadcast_in_dim.45), channel_id=1, replica_groups=mesh['sp'=64,'tp'=4] {'tp'}, dimensions={0} | all-to-all | bytes 4194304 | tf_op jit(solution)/shard_map/all_to_all | solution.py:29
  119.6 4.1 %all-to-all-start.5 = ((bf16[4,32,2048]{2,1,0:T(8,128)(2,1)}), bf16[4,32,2048]{2,1,0:T(8,128)(2,1)}, u32[]{:S(2)}, u32[]{:S(2)}) async-start(bf16[4,32,2048]{2,1,0:T(8,128)(2,1)} %broadcast_in_dim.46), calls=%async_computation.5 | async-start | bytes 1048576 | tf_op jit(solution)/shard_map/all_to_all | solution.py:29
  124.0 1.3 copy-done.1
  125.4 1.5 convolution_bitcast_fusion.1
  126.9 4.3 %convolution_convert_fusion = bf16[256,2,2048]{2,0,1:T(8,128)(2,1)S(1)} fusion(bf16[256,2,2048]{2,0,1:T(8,128)(2,1)} %bitcast.73, bf16[1,256,2048]{2,1,0:T(8,128)(2,1)S(1)} %copy-done, bf16[1,2048,256]{2,1,0:T(8,128)(2,1)} %param.27, f32[256,1,2,256]{3,0,2,1:T(8,128)} %convolution_bitcast_fusion.1), kind=kOutput, calls=%fused_computation.3 | convolution fusion | flops 1075576832 | bytes 6815744 | tf_op jit(solution)/shard_map/aecf,efd->aecd/dot_general | solution.py:374
  131.2 1.5 copy.30
  132.7 4.2 %all-to-all-start.3 = ((bf16[4,64,1,2,2048]{4,1,3,2,0:T(8,128)(2,1)}), bf16[4,64,1,2,2048]{4,1,3,2,0:T(8,128)(2,1)S(1)}, u32[]{:S(2)}, u32[]{:S(2)}) async-start(bf16[4,64,1,2,2048]{4,1,3,2,0:T(8,128)(2,1)} %copy.30), calls=%async_computation.3 | async-start | bytes 4194304 | tf_op jit(solution)/shard_map/all_to_all | solution.py:23
  136.9 1.7 fusion.30
  138.6 3.3 %convolution_convert_fusion.1 = bf16[128,2048]{1,0:T(8,128)(2,1)} fusion(bf16[256,2048]{1,0:T(8,128)(2,1)} %param.31, bf16[128,2048]{1,0:T(8,128)(2,1)} %bitcast.28, bf16[2048,256]{1,0:T(8,128)(2,1)} %param.30, f32[128,256]{1,0:T(8,128)S(1)} %fusion.30), kind=kOutput, calls=%fused_computation.4 | convolution fusion | flops 268894208 | bytes 3276800 | tf_op jit(solution)/shard_map/dot_general | solution.py:380
  141.9 19.6 %all-to-all-done.3 = bf16[4,64,1,2,2048]{4,1,3,2,0:T(8,128)(2,1)S(1)} async-done(((bf16[4,64,1,2,2048]{4,1,3,2,0:T(8,128)(2,1)}), bf16[4,64,1,2,2048]{4,1,3,2,0:T(8,128)(2,1)S(1)}, u32[]{:S(2)}, u32[]{:S(2)}) %all-to-all-start.3) | async-done | bytes 2097184 | tf_op jit(solution)/shard_map/all_to_all | solution.py:23
  161.5 4.1 %all-to-all-start.6 = ((bf16[4,32,2048]{2,1,0:T(8,128)(2,1)}), bf16[4,32,2048]{2,1,0:T(8,128)(2,1)}, u32[]{:S(2)}, u32[]{:S(2)}) async-start(bf16[4,32,2048]{2,1,0:T(8,128)(2,1)} %bitcast.71), calls=%async_computation.6 | async-start | bytes 1048576 | tf_op jit(solution)/shard_map/all_to_all | solution.py:23
  165.6 1.3 reduce_sum.96
  167.0 2.4 %copy.32 = bf16[64,1,2,2048]{3,2,1,0:T(2,128)(2,1)} copy(bf16[64,1,2,2048]{3,0,2,1:T(8,128)(2,1)} %bitcast.76) | data formatting | bytes 1048576 | tf_op jit(solution)/shard_map/reduce_sum | solution.py:24
  169.4 3.3 %all-to-all-done.6 = bf16[4,32,2048]{2,1,0:T(8,128)(2,1)} async-done(((bf16[4,32,2048]{2,1,0:T(8,128)(2,1)}), bf16[4,32,2048]{2,1,0:T(8,128)(2,1)}, u32[]{:S(2)}, u32[]{:S(2)}) %all-to-all-start.6) | async-done | bytes 524320 | tf_op jit(solution)/shard_map/all_to_all | solution.py:23
  172.6 8.8 %all-to-all-start.4 = ((bf16[64,1,2,2048]{3,2,1,0:T(2,128)(2,1)}), bf16[64,1,2,2048]{3,2,1,0:T(2,128)(2,1)S(1)}, u32[]{:S(2)}, u32[]{:S(2)}) async-start(bf16[64,1,2,2048]{3,2,1,0:T(2,128)(2,1)} %copy.32), calls=%async_computation.4 | async-start | bytes 1048576 | tf_op jit(solution)/shard_map/all_to_all | solution.py:385
  181.6 1.1 reduce_sum.99
  182.7 16.5 %all-to-all-done.4 = bf16[64,1,2,2048]{3,2,1,0:T(2,128)(2,1)S(1)} async-done(((bf16[64,1,2,2048]{3,2,1,0:T(2,128)(2,1)}), bf16[64,1,2,2048]{3,2,1,0:T(2,128)(2,1)S(1)}, u32[]{:S(2)}, u32[]{:S(2)}) %all-to-all-start.4) | async-done | bytes 524320 | tf_op jit(solution)/shard_map/all_to_all | solution.py:385
  (55 shorter events, 7.2 us)
Async XLA Ops:
  0.0 126.9 %copy-start = (bf16[1,256,2048]{2,1,0:T(8,128)(2,1)S(1)}, bf16[1,256,2048]{2,1,0:T(8,128)(2,1)}, u32[]{:S(2)}) copy-start(bf16[1,256,2048]{2,1,0:T(8,128)(2,1)} %param.28) | copy-start | bytes 3145732
  0.0 51.3 %copy-start.5 = (s32[32,2]{0,1:T(2,128)S(1)}, s32[32,2]{0,1:T(2,128)}, u32[]{:S(2)}) copy-start(s32[32,2]{0,1:T(2,128)} %param.24) | copy-start | bytes 772
  0.0 53.0 %copy-start.3 = (f32[2,2048]{1,0:T(2,128)S(1)}, f32[2,2048]{1,0:T(2,128)}, u32[]{:S(2)}) copy-start(f32[2,2048]{1,0:T(2,128)} %param.23) | copy-start | bytes 49156
  0.0 53.2 %copy-start.4 = (f32[2,2048]{1,0:T(2,128)S(1)}, f32[2,2048]{1,0:T(2,128)}, u32[]{:S(2)}) copy-start(f32[2,2048]{1,0:T(2,128)} %param.22) | copy-start | bytes 49156
  0.0 60.6 %copy-start.2 = (bf16[32,2048]{1,0:T(8,128)(2,1)S(1)}, bf16[32,2048]{1,0:T(8,128)(2,1)}, u32[]{:S(2)}) copy-start(bf16[32,2048]{1,0:T(8,128)(2,1)} %param.16) | copy-start | bytes 393220
  47.1 13.5 %all-to-all-start = ((bf16[4,32,2048]{2,1,0:T(8,128)(2,1)}), bf16[4,32,2048]{2,1,0:T(8,128)(2,1)S(1)}, u32[]{:S(2)}, u32[]{:S(2)}) async-start(bf16[4,32,2048]{2,1,0:T(8,128)(2,1)} %bitcast), calls=%async_computation | async-start | bytes 1048576 | tf_op jit(solution)/shard_map/all_to_all | solution.py:23
  119.6 13.0 %all-to-all-start.5 = ((bf16[4,32,2048]{2,1,0:T(8,128)(2,1)}), bf16[4,32,2048]{2,1,0:T(8,128)(2,1)}, u32[]{:S(2)}, u32[]{:S(2)}) async-start(bf16[4,32,2048]{2,1,0:T(8,128)(2,1)} %broadcast_in_dim.46), calls=%async_computation.5 | async-start | bytes 1048576 | tf_op jit(solution)/shard_map/all_to_all | solution.py:29
  123.8 1.6 copy-start.7
  123.9 1.4 copy-start.1
  132.7 28.8 %all-to-all-start.3 = ((bf16[4,64,1,2,2048]{4,1,3,2,0:T(8,128)(2,1)}), bf16[4,64,1,2,2048]{4,1,3,2,0:T(8,128)(2,1)S(1)}, u32[]{:S(2)}, u32[]{:S(2)}) async-start(bf16[4,64,1,2,2048]{4,1,3,2,0:T(8,128)(2,1)} %copy.30), calls=%async_computation.3 | async-start | bytes 4194304 | tf_op jit(solution)/shard_map/all_to_all | solution.py:23
  161.5 11.1 %all-to-all-start.6 = ((bf16[4,32,2048]{2,1,0:T(8,128)(2,1)}), bf16[4,32,2048]{2,1,0:T(8,128)(2,1)}, u32[]{:S(2)}, u32[]{:S(2)}) async-start(bf16[4,32,2048]{2,1,0:T(8,128)(2,1)} %bitcast.71), calls=%async_computation.6 | async-start | bytes 1048576 | tf_op jit(solution)/shard_map/all_to_all | solution.py:23
  165.6 15.8 %copy-start.6 = (f32[32,2]{0,1:T(2,128)S(1)}, f32[32,2]{0,1:T(2,128)}, u32[]{:S(2)}) copy-start(f32[32,2]{0,1:T(2,128)} %param.25) | copy-start | bytes 772
  172.6 26.5 %all-to-all-start.4 = ((bf16[64,1,2,2048]{3,2,1,0:T(2,128)(2,1)}), bf16[64,1,2,2048]{3,2,1,0:T(2,128)(2,1)S(1)}, u32[]{:S(2)}, u32[]{:S(2)}) async-start(bf16[64,1,2,2048]{3,2,1,0:T(2,128)(2,1)} %copy.32), calls=%async_computation.4 | async-start | bytes 1048576 | tf_op jit(solution)/shard_map/all_to_all | solution.py:385

commit v3 on v2

--- a/solution.py
+++ b/solution.py
@@ -10,42 +10,6 @@
 LOG2E = 1.4426950408889634
 ALPHA = 8.0**0.25
 LN_EPS = 1e-05
-
-
-def split_up(array, dim, peers):
-    dims = array.shape
-    blocks = array.reshape(*dims[:dim], peers, dims[dim] // peers, *dims[dim + 1 :])
-    return jnp.moveaxis(blocks, dim, 0)
-
-
-def summed_on_arrival(array, axis, dim):
-    peers = lax.axis_size(axis)
-    blocks = lax.all_to_all(split_up(array, dim, peers), axis, 0, 0, tiled=True)
-    return jnp.sum(blocks.astype(jnp.float32), axis=0)
-
-
-def sent_to_all(array, axis):
-    peers = lax.axis_size(axis)
-    return lax.all_to_all(
-        jnp.broadcast_to(array[None], (peers, *array.shape)), axis, 0, 0, tiled=True
-    )
-
-
-def joined_along(blocks, dim):
-    dims = list(blocks.shape[1:])
-    dims[dim] *= blocks.shape[0]
-    return jnp.moveaxis(blocks, 0, dim).reshape(dims)
-
-
-def collect(array, axis, dim):
-    blocks = sent_to_all(array, axis)
-    return joined_along(blocks, dim)
-
-
-def layer_norm(summed, gain, shift):
-    center = summed - jnp.mean(summed, axis=-1, keepdims=True)
-    spread = jnp.mean(center * center, axis=-1, keepdims=True)
-    return (center * lax.rsqrt(spread + LN_EPS) * gain + shift).astype(jnp.bfloat16)
 
 
 def cross(sp_count):
@@ -321,6 +285,343 @@
     )(offset, queries, keys, values)
 
 
+def moe_kernel(rows_z, chunks, capacity,
+               att_ref, res_ref, route_ref, rw_ref, gain_ref, bias_ref,
+               wo_hbm, wg_hbm, wu_hbm, wd_hbm, sg_hbm, su_hbm, sd_hbm,
+               out_ref,
+               wo, wg, wu, wd, sg, su, sd,
+               proj, proj_far, proj_in, normed, tokens,
+               out_z, in_z, out_x, rows_all, gate, up, shared_hidden, hidden,
+               part, part_far, part_in, back_x, in_bx, back_z, in_bz, shared_sum, total,
+               send, recv, local):
+    me = lax.axis_index("sp")
+    y = lax.axis_index("tp")
+    group = lax.axis_size("sp") // rows_z
+    z, w = lax.div(me, group), lax.rem(me, group)
+    tp = lax.axis_size("tp")
+    block = rows_z * capacity
+    rows, width = res_ref.shape
+    slots = out_z.shape[0]
+    cols = width // chunks
+    mesh_ids = pl.DeviceIdType.MESH
+
+    def turn(value, by, size):
+        return lax.rem(value + (by + size), size)
+
+    y_side = {1: turn(y, 1, tp), -1: turn(y, -1, tp)}
+    y_far = turn(y, 2, tp)
+
+    barrier = pltpu.get_barrier_semaphore()
+    peers = [{"sp": turn(z, d, rows_z) * group + w} for d in range(1, rows_z)]
+    peers += [{"sp": z * group + turn(w, d, group)} for d in range(1, group)]
+    peers += [{"tp": y_side[1]}, {"tp": y_side[-1]}]
+    for peer in peers:
+        pl.semaphore_signal(barrier, inc=1, device_id=peer, device_id_type=mesh_ids)
+
+    loads = []
+    for i, (src, dst) in enumerate((
+        (wo_hbm, wo), (sg_hbm, sg), (su_hbm, su), (wg_hbm.at[0], wg), (wu_hbm.at[0], wu),
+        (wd_hbm.at[0], wd), (sd_hbm, sd),
+    )):
+        load = pltpu.make_async_copy(src, dst, local.at[i])
+        load.start()
+        loads.append(load)
+
+    names = {}
+    started = []
+
+    def copy(name, src, dst, target):
+        slot = names.setdefault(name, len(names))
+        return pltpu.make_async_remote_copy(
+            src_ref=src, dst_ref=dst, send_sem=send.at[slot], recv_sem=recv.at[slot],
+            device_id=target, device_id_type=mesh_ids,
+        )
+
+    def begin(name, src, dst, target):
+        job = copy(name, src, dst, target)
+        job.start()
+        started.append(job)
+
+    def arrive(name, dst):
+        copy(name, dst, dst, {"tp": y_side[1]}).wait_recv()
+
+    def to_y(way):
+        return {"tp": y_side[way]}
+
+    loads[0].wait()
+    for j in range(tp):
+        proj[j] = jnp.dot(
+            att_ref[j * rows : (j + 1) * rows, :], wo[...], preferred_element_type=jnp.float32
+        ).astype(jnp.bfloat16)
+    pl.semaphore_wait(barrier, len(peers))
+
+    def halves(n):
+        return {1: pl.ds(0, n // 2), -1: pl.ds(n // 2, n // 2)}
+
+    def sum_far(tag, src, far, at):
+        piece = halves(src.shape[1])
+        for way in (1, -1):
+            begin((tag, "far", way), at(src.at[y_far, piece[way]]), at(far.at[0 if way == 1 else 1]), to_y(way))
+
+    def sum_pass(tag, src, far, arrived, at):
+        piece = halves(src.shape[1])
+        for way in (1, -1):
+            got = at(far.at[0 if way == 1 else 1])
+            arrive((tag, "far", way), got)
+            mine = at(src.at[y_side[way], piece[way]])
+            mine[...] = (mine[...].astype(jnp.float32) + got[...].astype(jnp.float32)).astype(jnp.bfloat16)
+            begin((tag, "near", way), at(src.at[y_side[way]]), at(arrived.at[0 if way == 1 else 1]), to_y(way))
+
+    def sum_done(tag, src, arrived, at):
+        acc = at(src.at[y])[...].astype(jnp.float32)
+        for way in (1, -1):
+            got = at(arrived.at[0 if way == 1 else 1])
+            arrive((tag, "near", way), got)
+            acc = acc + got[...].astype(jnp.float32)
+        return acc
+
+    def spread(tag, buf, at):
+        for way in (1, -1):
+            begin((tag, "near", way), at(buf.at[y]), at(buf.at[y]), to_y(way))
+
+    def spread_pass(tag, buf, at):
+        piece = halves(buf.shape[1])
+        for way in (1, -1):
+            side = y_side[-way]
+            arrive((tag, "near", way), at(buf.at[side]))
+            half = at(buf.at[side, piece[way]])
+            begin((tag, "far", way), half, half, to_y(way))
+
+    def spread_done(tag, buf, at):
+        piece = halves(buf.shape[1])
+        for way in (1, -1):
+            arrive((tag, "far", way), at(buf.at[y_far, piece[way]]))
+
+    def all_of(ref):
+        return ref
+
+    def chunk_of(q):
+        return lambda ref: ref.at[:, pl.ds(q * cols, cols)]
+
+    sum_far("proj", proj, proj_far, all_of)
+
+    t_row = lax.broadcasted_iota(jnp.int32, (rows, rows), 0)
+    t_col = lax.broadcasted_iota(jnp.int32, (rows, rows), 1)
+    routes = route_ref[...].astype(jnp.float32)
+    e_col = [routes[:, k : k + 1] for k in (0, 1)]
+    e_row = [jnp.sum(jnp.where(t_row == t_col, e, 0.0), axis=0, keepdims=True) for e in e_col]
+
+    def same(a, b, keep=None):
+        hit = jnp.where(a == b, 1.0, 0.0)
+        return hit if keep is None else jnp.where(keep, hit, 0.0)
+
+    rank_col = [
+        jnp.sum(same(e_col[0], e_row[0], t_col < t_row), axis=1, keepdims=True),
+        jnp.sum(same(e_col[1], e_row[0]) + same(e_col[1], e_row[1], t_col < t_row), axis=1, keepdims=True),
+    ]
+    rank_row = [
+        jnp.sum(same(e_col[0], e_row[0], t_row < t_col), axis=0, keepdims=True),
+        jnp.sum(same(e_col[0], e_row[1]) + same(e_col[1], e_row[1], t_row < t_col), axis=0, keepdims=True),
+    ]
+    slot_col = [e_col[k] * capacity + rank_col[k] for k in (0, 1)]
+    slot_row = [e_row[k] * capacity + rank_row[k] for k in (0, 1)]
+    s_row = lax.broadcasted_iota(jnp.int32, (slots, rows), 0).astype(jnp.float32)
+    place = (same(s_row, slot_row[0]) + same(s_row, slot_row[1])).astype(jnp.bfloat16)
+    s_col = lax.broadcasted_iota(jnp.int32, (rows, slots), 1).astype(jnp.float32)
+    pick = [same(s_col, slot_col[k]).astype(jnp.bfloat16) for k in (0, 1)]
+    i_dst = lax.broadcasted_iota(jnp.int32, (slots, slots), 0)
+    i_src = lax.broadcasted_iota(jnp.int32, (slots, slots), 1)
+    from_row = lax.div(lax.rem(i_dst, block), capacity) * block + lax.div(i_dst, block) * capacity + lax.rem(i_dst, capacity)
+    swap = jnp.where(i_src == from_row, 1.0, 0.0).astype(jnp.bfloat16)
+
+    def norm(summed, n):
+        center = summed - jnp.mean(summed, axis=-1, keepdims=True)
+        spread_ = jnp.mean(center * center, axis=-1, keepdims=True)
+        scaled = center * lax.rsqrt(spread_ + LN_EPS) * gain_ref[n : n + 1, :] + bias_ref[n : n + 1, :]
+        return scaled.astype(jnp.bfloat16)
+
+    sum_pass("proj", proj, proj_far, proj_in, all_of)
+    mixed = sum_done("proj", proj, proj_in, all_of)
+    normed[...] = norm(ALPHA * res_ref[...].astype(jnp.float32) + mixed, 0)
+    tokens[y] = normed[...]
+
+    def rows_at(n):
+        return pl.ds(pl.multiple_of(n * block, block), block)
+
+    def exchange(tag, q, axis, outgoing, incoming):
+        here, size = (z, rows_z) if axis == "z" else (w, group)
+        span = pl.ds(q * cols, cols)
+        for d in range(1, size):
+            there = turn(here, d, size)
+            target = {"sp": there * group + w} if axis == "z" else {"sp": z * group + there}
+            begin((tag, q, d), outgoing.at[rows_at(there), span], incoming.at[rows_at(here), span], target)
+        incoming[rows_at(here), span] = outgoing[rows_at(here), span]
+
+    def exchanged(tag, q, axis, incoming):
+        here, size = (z, rows_z) if axis == "z" else (w, group)
+        for d in range(1, size):
+            arrive((tag, q, d), incoming.at[rows_at(turn(here, -d, size)), pl.ds(q * cols, cols)])
+
+    def moved(matrix, value):
+        return jnp.dot(matrix, value, preferred_element_type=jnp.float32).astype(jnp.bfloat16)
+
+    def span_of(q):
+        return slice(q * cols, (q + 1) * cols)
+
+    def d0(q):
+        out_z[:, span_of(q)] = moved(place, normed[:, span_of(q)])
+        exchange("dz", q, "z", out_z, in_z)
+
+    def d1(q):
+        exchanged("dz", q, "z", in_z)
+        out_x[:, span_of(q)] = moved(swap, in_z[:, span_of(q)])
+        exchange("dx", q, "x", out_x, rows_all.at[y])
+
+    def d2(q):
+        exchanged("dx", q, "x", rows_all.at[y])
+        spread(("dy", q), rows_all, chunk_of(q))
+
+    def d3(q):
+        spread_pass(("dy", q), rows_all, chunk_of(q))
+
+    def d4(q):
+        spread_done(("dy", q), rows_all, chunk_of(q))
+        x = rows_all[:, :, span_of(q)].reshape(tp * slots, cols)
+        if q == 0:
+            loads[3].wait()
+            loads[4].wait()
+        g = jnp.dot(x, wg[span_of(q), :], preferred_element_type=jnp.float32)
+        u = jnp.dot(x, wu[span_of(q), :], preferred_element_type=jnp.float32)
+        gate[...] = g if q == 0 else gate[...] + g
+        up[...] = u if q == 0 else up[...] + u
+
+    def act(g, u):
+        return (g / (1.0 + jnp.exp(-g)) * u).astype(jnp.bfloat16)
+
+    def shared_in():
+        spread_done("tok", tokens, all_of)
+        loads[1].wait()
+        loads[2].wait()
+        x = tokens[...].reshape(tp * rows, width)
+        g = jnp.dot(x, sg[...], preferred_element_type=jnp.float32)
+        u = jnp.dot(x, su[...], preferred_element_type=jnp.float32)
+        shared_hidden[...] = act(g, u)
+
+    def e0(q):
+        p = jnp.dot(hidden[...], wd[:, span_of(q)], preferred_element_type=jnp.float32)
+        part[:, :slots, span_of(q)] = p.astype(jnp.bfloat16).reshape(tp, slots, cols)
+        s = jnp.dot(shared_hidden[...], sd[:, span_of(q)], preferred_element_type=jnp.float32)
+        part[:, slots:, span_of(q)] = s.astype(jnp.bfloat16).reshape(tp, rows, cols)
+        sum_far(("ry", q), part, part_far, chunk_of(q))
+
+    def e1(q):
+        sum_pass(("ry", q), part, part_far, part_in, chunk_of(q))
+
+    def e2(q):
+        acc = sum_done(("ry", q), part, part_in, chunk_of(q)).astype(jnp.bfloat16)
+        back_x[:, span_of(q)] = acc[:slots]
+        shared_sum[:, span_of(q)] = acc[slots:]
+        exchange("rx", q, "x", back_x, in_bx)
+
+    def e3(q):
+        exchanged("rx", q, "x", in_bx)
+        back_z[:, span_of(q)] = moved(swap, in_bx[:, span_of(q)])
+        exchange("rz", q, "z", back_z, in_bz)
+
+    def e4(q):
+        exchanged("rz", q, "z", in_bz)
+        got = in_bz[:, span_of(q)]
+        routed = [
+            jnp.dot(pick[k], got, preferred_element_type=jnp.float32) * rw_ref[:, k : k + 1]
+            for k in (0, 1)
+        ]
+        combined = routed[0] + routed[1] + shared_sum[:, span_of(q)].astype(jnp.float32)
+        total[:, span_of(q)] = ALPHA * normed[:, span_of(q)].astype(jnp.float32) + combined
+
+    d0(0)
+    spread("tok", tokens, all_of)
+    for q in range(1, chunks):
+        d0(q)
+
+    def pipeline(stages, extra):
+        for at in range(chunks + len(stages) - 1):
+            for s, stage in enumerate(stages):
+                if 0 <= at - s < chunks:
+                    stage(at - s)
+            if at in extra:
+                extra[at]()
+
+    pipeline((d1, d2, d3, d4), {0: lambda: spread_pass("tok", tokens, all_of), 1: shared_in})
+    hidden[...] = act(gate[...], up[...])
+    loads[5].wait()
+    loads[6].wait()
+    pipeline((e0, e1, e2, e3, e4), {})
+    out_ref[...] = norm(total[...], 1)
+    for job in started:
+        job.wait_send()
+
+
+def moe(attended, residual, routing, route_weight, norm_gain, norm_bias, w_out,
+        w_exp_gate, w_exp_up, w_exp_down, w_shared_gate, w_shared_up, w_shared_down):
+    rows, width = residual.shape
+    tp = lax.axis_size("tp")
+    sp = lax.axis_size("sp")
+    rows_z, _ = cross(sp)
+    capacity = 2
+    slots = sp * capacity
+    ff = w_exp_gate.shape[2]
+    bf16, f32 = jnp.bfloat16, jnp.float32
+    vmem = pl.BlockSpec(memory_space=pltpu.VMEM)
+    hbm = pl.BlockSpec(memory_space=pl.ANY)
+    both = slots + rows
+    scratch = [
+        pltpu.VMEM(w_out.shape, bf16),
+        pltpu.VMEM((width, ff), bf16),
+        pltpu.VMEM((width, ff), bf16),
+        pltpu.VMEM((ff, width), bf16),
+        pltpu.VMEM(w_shared_gate.shape, bf16),
+        pltpu.VMEM(w_shared_up.shape, bf16),
+        pltpu.VMEM(w_shared_down.shape, bf16),
+        pltpu.VMEM((tp, rows, width), bf16),
+        pltpu.VMEM((2, rows // 2, width), bf16),
+        pltpu.VMEM((2, rows, width), bf16),
+        pltpu.VMEM((rows, width), bf16),
+        pltpu.VMEM((tp, rows, width), bf16),
+        pltpu.VMEM((slots, width), bf16),
+        pltpu.VMEM((slots, width), bf16),
+        pltpu.VMEM((slots, width), bf16),
+        pltpu.VMEM((tp, slots, width), bf16),
+        pltpu.VMEM((tp * slots, ff), f32),
+        pltpu.VMEM((tp * slots, ff), f32),
+        pltpu.VMEM((tp * rows, w_shared_gate.shape[1]), bf16),
+        pltpu.VMEM((tp * slots, ff), bf16),
+        pltpu.VMEM((tp, both, width), bf16),
+        pltpu.VMEM((2, both // 2, width), bf16),
+        pltpu.VMEM((2, both, width), bf16),
+        pltpu.VMEM((slots, width), bf16),
+        pltpu.VMEM((slots, width), bf16),
+        pltpu.VMEM((slots, width), bf16),
+        pltpu.VMEM((slots, width), bf16),
+        pltpu.VMEM((rows, width), bf16),
+        pltpu.VMEM((rows, width), f32),
+        pltpu.SemaphoreType.DMA((192,)),
+        pltpu.SemaphoreType.DMA((192,)),
+        pltpu.SemaphoreType.DMA((7,)),
+    ]
+    return pl.pallas_call(
+        functools.partial(moe_kernel, rows_z, 4, capacity),
+        out_shape=jax.ShapeDtypeStruct((rows, width), bf16),
+        in_specs=[vmem] * 6 + [hbm] * 7,
+        out_specs=vmem,
+        scratch_shapes=scratch,
+        compiler_params=pltpu.CompilerParams(
+            collective_id=1, has_side_effects=True, vmem_limit_bytes=48 * 1024 * 1024
+        ),
+        name="moe",
+    )(attended, residual, routing, route_weight, norm_gain, norm_bias, w_out,
+      w_exp_gate, w_exp_up, w_exp_down, w_shared_gate, w_shared_up, w_shared_down)
+
+
 def per_device(
     residual,
     query_rows,
@@ -339,58 +640,11 @@
     w_shared_up,
     w_shared_down,
 ):
-    sp_count = lax.axis_size("sp")
     attended = attend(head_offset, query_rows, key_rows, value_rows)
-    rows_local = residual.shape[0]
-    mixed = summed_on_arrival(
-        jnp.dot(attended, w_out, preferred_element_type=jnp.float32).astype(jnp.bfloat16), "tp", 0
+    return moe(
+        attended, residual, routing, route_weight, norm_gain, norm_bias, w_out,
+        w_exp_gate, w_exp_up, w_exp_down, w_shared_gate, w_shared_up, w_shared_down,
     )
-    normed = layer_norm(ALPHA * residual.astype(jnp.float32) + mixed, norm_gain[0], norm_bias[0])
-    top_k = routing.shape[1]
-    exp_local = w_exp_gate.shape[0]
-    experts = exp_local * sp_count
-    capacity = max(2, 3 * rows_local * top_k // (2 * experts))
-    flat_routes = routing.reshape(-1)
-    one_hot = (flat_routes[:, None] == jnp.arange(experts, dtype=jnp.int32)[None, :]).astype(
-        jnp.int32
-    )
-    slot_rank = jnp.sum((jnp.cumsum(one_hot, axis=0) - 1) * one_hot, axis=1)
-    slot_index = flat_routes * capacity + slot_rank
-    pair_token = jnp.arange(flat_routes.shape[0], dtype=jnp.int32) // top_k
-    source_row = (
-        jnp.full((experts * capacity,), rows_local, jnp.int32).at[slot_index].set(pair_token)
-    )
-    outgoing = jnp.take(normed, source_row, axis=0, mode="fill", fill_value=0)
-    outgoing = outgoing.reshape(sp_count, exp_local, capacity, -1)
-    arrived = lax.all_to_all(outgoing, "sp", split_axis=0, concat_axis=0, tiled=True)
-    routed_rows, token_rows = (collect(arrived, "tp", 0), collect(normed, "tp", 0))
-    gate_part = jnp.einsum(
-        "aecd,edf->aecf", routed_rows, w_exp_gate, preferred_element_type=jnp.float32
-    )
-    up_part = jnp.einsum(
-        "aecd,edf->aecf", routed_rows, w_exp_up, preferred_element_type=jnp.float32
-    )
-    hidden = (jax.nn.silu(gate_part) * up_part).astype(jnp.bfloat16)
-    expert_part = jnp.einsum(
-        "aecf,efd->aecd", hidden, w_exp_down, preferred_element_type=jnp.float32
-    )
-    shared_gate = jnp.dot(token_rows, w_shared_gate, preferred_element_type=jnp.float32)
-    shared_up = jnp.dot(token_rows, w_shared_up, preferred_element_type=jnp.float32)
-    shared_hidden = (jax.nn.silu(shared_gate) * shared_up).astype(jnp.bfloat16)
-    shared_part = jnp.dot(shared_hidden, w_shared_down, preferred_element_type=jnp.float32)
-    expert_sum, shared_sum = (
-        summed_on_arrival(expert_part.astype(jnp.bfloat16), "tp", 0),
-        summed_on_arrival(shared_part.astype(jnp.bfloat16), "tp", 0),
-    )
-    returned = lax.all_to_all(
-        expert_sum.astype(jnp.bfloat16), "sp", split_axis=0, concat_axis=0, tiled=True
-    )
-    returned = returned.reshape(experts * capacity, -1)
-    picked = returned[slot_index].astype(jnp.float32).reshape(rows_local, top_k, -1)
-    routed = jnp.sum(picked * route_weight[:, :, None], axis=1)
-    shared_out = lax.optimization_barrier(shared_sum.astype(jnp.bfloat16))
-    combined = routed + shared_out.astype(jnp.float32)
-    return layer_norm(ALPHA * normed.astype(jnp.float32) + combined, norm_gain[1], norm_bias[1])
 
 
 def solution(mesh):

time: 203 us -> 141 us (0.69)
  Pallas kernels: 44.7 us -> 132 us
  blocking collectives: 55.4 us -> 0 us
  waiting for transfers between devices: 46.6 us -> 0 us
  starting transfers between devices: 25.5 us -> 0 us
  matrix products: 13.1 us -> 0 us
  other arithmetic: 5.84 us -> 0 us
  local copies, waits for them, and re-layouts: 10.9 us -> 8.51 us
    pallas_call x0 -> x1, Pallas kernels: none -> 87.4 us  [moe(): pl.pallas_call(functools.partial(moe_kernel, rows_z, 4, capacity), out_sh...]
    all_to_all x2 -> x0, blocking collectives: 55.4 us -> none  [the longest x1 28.5 us: sent_to_all(): lax.all_to_all(jnp.broadcast_to(array[None], (peers, *array.shape)), axis...]
    all_to_all x5 -> x0, waiting for transfers between devices: 46.6 us -> none  [the longest x3 30.2 us: summed_on_arrival(): blocks = lax.all_to_all(split_up(array, dim, peers), axis, 0, 0, tiled=True)]
    all_to_all x5 -> x0, starting transfers between devices: 25.5 us -> none  [the longest x3 12.5 us: summed_on_arrival(): blocks = lax.all_to_all(split_up(array, dim, peers), axis, 0, 0, tiled=True)]
    dot_general x5 -> x0, matrix products: 13.1 us -> none  [the longest x1 4.29 us: per_device(): jnp.einsum('aecf,efd->aecd', hidden, w_exp_down, preferred_element_type=j...]
    unnamed x18 -> x23, local copies, waits for them, and re-layouts: 1.62 us -> 8.51 us
    reduce_sum x9 -> x0, other arithmetic: 4.17 us -> none  [the longest x3 2.54 us: summed_on_arrival(): return jnp.sum(blocks.astype(jnp.float32), axis=0)]
    reduce_sum x1 -> x0, local copies, waits for them, and re-layouts: 2.39 us -> none  [summed_on_arrival(): return jnp.sum(blocks.astype(jnp.float32), axis=0)]
  transfers between devices with their start and end apart: 5 -> 0, of which waited for: 4 -> 0; matrix products, arithmetic and copies ran while one was open for 10% -> 0% of each run, Pallas kernels for 0% -> 0%
where the time goes in v3:
time: 141 us
  Pallas kernels  132 us (94%)
  local copies, waits for them, and re-layouts  8.51 us (6%)
    pallas_call x1, Pallas kernels, moe(): pl.pallas_call(functools.partial(moe_kernel, rows_z, 4, capacity), out_sh...  87.4 us
    pallas_call x1, Pallas kernels, attend(): pl.pallas_call(functools.partial(attend_kernel, rows_z, rows_x), out_shap...  44.6 us
    unnamed x23, local copies, waits for them, and re-layouts  8.51 us

profile of v3, /device:TPU:1, one launch (start us, length us, event | category | flops | bytes accessed | tf_op | source)
XLA Modules:
  0.0 140.5 jit_solution(1428559371889480969)
XLA Ops:
  0.0 0.0 copy-start.9
  0.0 0.0 copy-start.6
  0.0 0.8 copy.17.route_ref
  0.8 0.0 copy-done.9
  0.8 0.1 copy.18.rw_ref
  0.9 0.0 copy-start.7
  0.9 0.0 copy-start.8
  0.9 44.6 %attend.1.att_ref = bf16[128,256]{1,0:T(8,128)(2,1)} custom-call(f32[2]{0:T(128)} %off_ref.1, bf16[128,256]{1,0:T(8,128)(2,1)} %q_ref.1, bf16[128,128]{1,0:T(8,128)(2,1)} %k_ref.1, bf16[128,128]{1,0:T(8,128)(2,1)} %v_ref.1), custom_call_target="tpu_custom_call" | custom-call | tf_op jit(solution)/shard_map/attend/pallas_call | solution.py:268
  45.5 0.0 copy-done.6
  45.5 0.0 copy-done.7
  45.5 0.0 copy-done.8
  45.5 0.0 copy-start
  45.5 1.2 copy-done
  46.7 0.0 copy-start.1
  46.8 1.2 copy-done.1
  48.0 1.2 copy-done.2
  49.2 0.0 copy-start.3
  49.2 1.2 copy-done.3
  50.4 0.0 copy-start.4
  50.4 1.2 copy-done.4
  51.6 0.0 copy-start.5
  51.7 0.8 copy-done.5
  52.5 87.4 %moe.1 = bf16[32,2048]{1,0:T(8,128)(2,1)S(1)} custom-call(bf16[128,256]{1,0:T(8,128)(2,1)S(1)} %copy-done.5, bf16[32,2048]{1,0:T(8,128)(2,1)S(1)} %copy-done.6, s32[32,2]{1,0:T(8,128)S(1)} %copy.17.route_ref, f32[32,2]{1,0:T(8,128)S(1)} %copy.18.rw_ref, f32[2,2048]{1,0:T(2,128)S(1)} %copy-done.7, f32[2,2048]{1,0:T(2,128)S(1)} %copy-done.8, ...), custom_call_target="tpu_custom_call" | custom-call | tf_op jit(solution)/shard_map/moe/pallas_call | solution.py:611
  139.9 0.7 copy.20
  (1 shorter events, 0.0 us)
Async XLA Ops:
  0.0 0.8 copy-start.9
  0.0 45.5 %copy-start.6 = (bf16[32,2048]{1,0:T(8,128)(2,1)S(1)}, bf16[32,2048]{1,0:T(8,128)(2,1)}, u32[]{:S(2)}) copy-start(bf16[32,2048]{1,0:T(8,128)(2,1)} %res_ref.1) | copy-start | bytes 393220
  0.9 44.6 %copy-start.7 = (f32[2,2048]{1,0:T(2,128)S(1)}, f32[2,2048]{1,0:T(2,128)}, u32[]{:S(2)}) copy-start(f32[2,2048]{1,0:T(2,128)} %gain_ref.1) | copy-start | bytes 49156
  0.9 44.6 %copy-start.8 = (f32[2,2048]{1,0:T(2,128)S(1)}, f32[2,2048]{1,0:T(2,128)}, u32[]{:S(2)}) copy-start(f32[2,2048]{1,0:T(2,128)} %bias_ref.1) | copy-start | bytes 49156
  45.5 1.2 copy-start
  46.7 1.2 copy-start.1
  48.0 1.2 copy-start.2
  49.2 1.2 copy-start.3
  50.4 1.2 copy-start.4
  51.6 0.8 copy-start.5

commit v4 on v1

v4 whole, which is shorter than its diff:
```python
import functools

import jax
import jax.numpy as jnp
from jax import lax
from jax.experimental import pallas as pl
from jax.experimental.pallas import tpu as pltpu
from jax.sharding import PartitionSpec as P

LOG2E = 1.4426950408889634
ALPHA = 8.0**0.25
LN_EPS = 1e-05


def cross(sp_count):
    rows_x = 4
    return sp_count // (2 * rows_x), rows_x


def layer_kernel(rows_z, rows_x, chunks, capacity,
                 off_ref, q_ref, k_ref, v_ref, res_ref, route_ref, rw_ref, gain_ref, bias_ref,
                 wo_hbm, wg_hbm, wu_hbm, wd_hbm, sg_hbm, su_hbm, sd_hbm,
                 out_ref,
                 keys, values, right, left, carry,
                 wo, wg, wu, wd, sg, su, sd,
                 proj, proj_in, normed, tokens,
                 out_z, in_z, out_x, rows_all, gate, up, shared_hidden, hidden, hidden_in,
                 part, part_far, part_in, back_x, in_bx, back_z, in_bz, total,
                 send, recv, local):
    me = lax.axis_index("sp")
    y = lax.axis_index("tp")
    tp = lax.axis_size("tp")
    group = 2 * rows_x
    z, w = lax.div(me, group), lax.rem(me, group)
    x, c = lax.div(w, 2), lax.rem(w, 2)
    q_rows = q_ref.shape[0]
    heads = off_ref.shape[0]
    dh = k_ref.shape[1]
    reach = rows_z // 2
    block = rows_z * capacity
    rows, width = res_ref.shape
    slots = out_z.shape[0]
    cols = width // chunks
    mesh_ids = pl.DeviceIdType.MESH

    def turn(value, by, size):
        return lax.rem(value + (by + size), size)

    def at(zz, xx, cc):
        return {"sp": (zz * rows_x + xx) * 2 + cc}

    y_side = {1: turn(y, 1, tp), -1: turn(y, -1, tp), 2: turn(y, 2, tp)}
    x_side = {1: turn(x, 1, rows_x), -1: turn(x, -1, rows_x), 2: turn(x, 2, rows_x)}
    to_z = {way: at(turn(z, way, rows_z), x, c) for way in (1, -1)}
    to_x = {way: at(z, x_side[way], c) for way in (1, -1, 2)}
    to_y = {way: {"tp": y_side[way]} for way in (1, -1, 2)}
    partner = at(z, x, 1 - c)
    ways = (1, -1)
    every_way = (2, 1, -1)

    barrier = pltpu.get_barrier_semaphore()
    peers = [{"sp": turn(z, d, rows_z) * group + w} for d in range(1, rows_z)]
    peers += [{"sp": z * group + turn(w, d, group)} for d in range(1, group)]
    peers += [to_y[way] for way in every_way]
    for peer in peers:
        pl.semaphore_signal(barrier, inc=1, device_id=peer, device_id_type=mesh_ids)

    loads = []
    for i, (src, dst) in enumerate((
        (wd_hbm.at[0], wd.at[y]), (wo_hbm, wo), (sg_hbm, sg), (su_hbm, su),
        (wg_hbm.at[0], wg), (wu_hbm.at[0], wu), (sd_hbm, sd),
        (k_ref, keys.at[z, x, c]), (v_ref, values.at[z, x, c]),
    )):
        load = pltpu.make_async_copy(src, dst, local.at[i])
        load.start()
        loads.append(load)

    names = {}
    started = []

    def copy(name, src, dst, target):
        slot = names.setdefault(name, len(names))
        return pltpu.make_async_remote_copy(
            src_ref=src, dst_ref=dst, send_sem=send.at[slot], recv_sem=recv.at[slot],
            device_id=target, device_id_type=mesh_ids,
        )

    def begin(name, src, dst, target):
        job = copy(name, src, dst, target)
        job.start()
        started.append(job)

    def arrive(name, dst):
        copy(name, dst, dst, partner).wait_recv()

    def halves(n):
        return {1: pl.ds(0, n // 2), -1: pl.ds(n // 2, n // 2)}

    def span(q):
        return pl.ds(q * cols, cols)

    def span_of(q):
        return slice(q * cols, (q + 1) * cols)

    pl.semaphore_wait(barrier, len(peers))

    own_k, own_v = keys.at[z, x, c], values.at[z, x, c]
    column = {"own": x, "down": x_side[-1], "up": x_side[1], "far": x_side[2]}
    last_way = {"own": 1, "down": 1, "up": -1, "far": -1}
    v_part = halves(q_rows)

    def slab_of(way, step):
        return turn(z, -way * step, rows_z)

    def slabs_at(step):
        if step == 0:
            return ((0, 0),)
        if step == reach:
            return ((1, step),)
        return ((1, step), (-1, step))

    def send_k(way, step, name):
        if step == reach and last_way[name] != way:
            return
        block_ = keys.at[slab_of(way, step - 1), column[name], c]
        src = k_ref if (step == 1 and name == "own") else block_
        begin(("kz", way, step, name), src, block_, to_z[way])

    def pass_k(step, name):
        if not 1 <= step <= reach:
            return
        for way in ways:
            if step == reach and last_way[name] != way:
                continue
            arrive(("kz", way, step, name), keys.at[slab_of(way, step), column[name], c])
            if step < reach:
                send_k(way, step + 1, name)

    def pass_v(step):
        for way in ways:
            zz = slab_of(way, step)
            if step < reach:
                block_ = values.at[zz, x, c]
                arrive(("vz", way, step), block_)
                piece = block_ if step + 1 < reach else values.at[zz, x, c, v_part[way]]
                begin(("vz", way, step + 1), piece, piece, to_z[way])
                for side in every_way:
                    begin(("vx", way, step, side), block_, block_, to_x[side])
            else:
                arrive(("vz", way, step), values.at[zz, x, c, v_part[way]])
        if step == reach:
            block_ = values.at[slab_of(1, step), x, c]
            for side in every_way:
                begin(("vx", 1, step, side), block_, block_, to_x[side])

    def from_x(tag, buf, zz):
        for side in (1, -1, 2):
            arrive(tag + (side,), buf.at[zz, x_side[2 if side == 2 else -side], c])

    def share(tag, buf, zz):
        begin(tag + ("peer",), buf.at[zz, :, c], buf.at[zz, :, c], partner)

    def shared(tag, buf, zz):
        arrive(tag + ("peer",), buf.at[zz, :, 1 - c])

    for way in every_way:
        begin(("kx", way), k_ref, own_k, to_x[way])
    for way in ways:
        send_k(way, 1, "own")
    for way in ways:
        begin(("vz", way, 1), v_ref, own_v, to_z[way])
    for way in every_way:
        begin(("vx", 0, 0, way), v_ref, own_v, to_x[way])
    for q in range(chunks):
        for way in ways:
            begin(("wd", q, way), wd_hbm.at[0, :, span(q)], wd.at[y, :, span(q)], to_y[way])

    def relay_down(q):
        piece = halves(wd.shape[1])
        for way in ways:
            side = y_side[-way]
            arrive(("wd", q, way), wd.at[side, :, span(q)])
            half = wd.at[side, piece[way], span(q)]
            begin(("wd", q, "far", way), half, half, to_y[way])

    def relayed_down(q):
        piece = halves(wd.shape[1])
        for way in ways:
            arrive(("wd", q, "far", way), wd.at[y_side[2], piece[way], span(q)])

    loads[7].wait()
    loads[8].wait()

    scale2 = dh**-0.5 * LOG2E
    sub = 2 * q_rows
    r_at = lax.broadcasted_iota(jnp.int32, (sub, sub), 0)
    c_at = lax.broadcasted_iota(jnp.int32, (sub, sub), 1)
    after_of = jnp.where(r_at > c_at, 1.0, 0.0).astype(jnp.bfloat16)
    t_in_slab = w * q_rows + lax.broadcasted_iota(jnp.int32, (q_rows, sub), 0)

    def slab(zz, carries, masked):
        stage = []
        for j in reversed(range(rows_x)):
            k = keys[zz, j].reshape(sub, dh)
            v = values[zz, j].reshape(sub, dh)
            mask = None
            if masked:
                mask = j * sub + lax.broadcasted_iota(jnp.int32, (q_rows, sub), 1) < t_in_slab
            for h in range(heads):
                q = q_ref[:, h * dh : (h + 1) * dh]
                s = lax.dot_general(q, k, (((1,), (1,)), ((), ())), preferred_element_type=jnp.float32)
                s = s * scale2 + off_ref[h] * LOG2E
                sp = jnp.maximum(s, 0.0) + jnp.log2(1.0 + jnp.exp2(-jnp.abs(s)))
                own = s - sp
                if masked:
                    sp = jnp.where(mask, sp, 0.0)
                hi = sp.astype(jnp.bfloat16)
                lo = (sp - hi.astype(jnp.float32)).astype(jnp.bfloat16)
                after = jnp.dot(hi, after_of, preferred_element_type=jnp.float32)
                after = after + jnp.dot(lo, after_of, preferred_element_type=jnp.float32)
                stage.append((h, own - after, after[:, :1] + sp[:, :1], v, mask))
        carries = list(carries)
        parts = [None] * heads
        for h, exponent, total_, v, mask in stage:
            weight = jnp.exp2(exponent - carries[h])
            if masked:
                weight = jnp.where(mask, weight, 0.0)
            piece = jnp.dot(weight.astype(jnp.bfloat16), v, preferred_element_type=jnp.float32)
            parts[h] = piece if parts[h] is None else parts[h] + piece
            carries[h] = carries[h] + total_
        return parts, carries

    def head_cols(h):
        return slice(h * dh, (h + 1) * dh)

    def put_carry(carries):
        for h in range(heads):
            carry[h] = jnp.broadcast_to(carries[h], (q_rows, dh))

    no_carry = [jnp.zeros((q_rows, 1), jnp.float32)] * heads

    def own_slab():
        parts, carries = slab(z, no_carry, True)
        for h in range(heads):
            right[:, head_cols(h)] = parts[h]
        put_carry(carries)
        left[...] = jnp.zeros_like(left)

    def right_slab(step):
        @pl.when(z >= step)
        def _():
            parts, carries = slab(z - step, [carry[h][:, :1] for h in range(heads)], False)
            for h in range(heads):
                right[:, head_cols(h)] = right[:, head_cols(h)] + parts[h]
            put_carry(carries)

    def left_slab(step):
        @pl.when(z + step >= rows_z)
        def _():
            parts, totals = slab(z + step - rows_z, no_carry, False)
            for h in range(heads):
                left[:, head_cols(h)] = parts[h] + jnp.exp2(-totals[h]) * left[:, head_cols(h)]

    def attend_slabs(step):
        for way, stp in slabs_at(step):
            shared(("k", way, stp), keys, slab_of(way, stp))
            shared(("v", way, stp), values, slab_of(way, stp))
        if step == 0:
            own_slab()
        else:
            right_slab(step)
            if step < reach:
                left_slab(step)

    for wave in range(1, reach + 2):
        pass_k(wave, "own")
        if wave == 1:
            from_x(("kx",), keys, z)
            for name in ("down", "up", "far"):
                for way in ways:
                    send_k(way, 1, name)
        else:
            for name in ("down", "up", "far"):
                pass_k(wave - 1, name)
        if wave <= reach:
            pass_v(wave)
        for way, stp in slabs_at(wave - 1):
            share(("k", way, stp), keys, slab_of(way, stp))
            from_x(("vx", way, stp), values, slab_of(way, stp))
            share(("v", way, stp), values, slab_of(way, stp))
        if 2 <= wave < chunks + 1:
            relay_down(wave - 2)
        if wave >= 2:
            attend_slabs(wave - 2)
    attend_slabs(reach)

    att = jnp.concatenate(
        [
            (right[:, head_cols(h)] + jnp.exp2(-carry[h]) * left[:, head_cols(h)]).astype(jnp.bfloat16)
            for h in range(heads)
        ],
        axis=1,
    )
    loads[1].wait()
    out_part = jnp.dot(att, wo[...], preferred_element_type=jnp.float32).astype(jnp.bfloat16)
    proj[...] = out_part.reshape(tp, rows, width)
    for way in every_way:
        begin(("proj", way), proj.at[y_side[way]], proj_in.at[y], to_y[way])

    t_row = lax.broadcasted_iota(jnp.int32, (rows, rows), 0)
    t_col = lax.broadcasted_iota(jnp.int32, (rows, rows), 1)
    routes = route_ref[...].astype(jnp.float32)
    e_col = [routes[:, k : k + 1] for k in (0, 1)]
    e_row = [jnp.sum(jnp.where(t_row == t_col, e, 0.0), axis=0, keepdims=True) for e in e_col]

    def same(a, b, keep=None):
        hit = jnp.where(a == b, 1.0, 0.0)
        return hit if keep is None else jnp.where(keep, hit, 0.0)

    rank_col = [
        jnp.sum(same(e_col[0], e_row[0], t_col < t_row), axis=1, keepdims=True),
        jnp.sum(same(e_col[1], e_row[0]) + same(e_col[1], e_row[1], t_col < t_row), axis=1, keepdims=True),
    ]
    rank_row = [
        jnp.sum(same(e_col[0], e_row[0], t_row < t_col), axis=0, keepdims=True),
        jnp.sum(same(e_col[0], e_row[1]) + same(e_col[1], e_row[1], t_row < t_col), axis=0, keepdims=True),
    ]
    slot_col = [e_col[k] * capacity + rank_col[k] for k in (0, 1)]
    slot_row = [e_row[k] * capacity + rank_row[k] for k in (0, 1)]
    s_row = lax.broadcasted_iota(jnp.int32, (slots, rows), 0).astype(jnp.float32)
    place = (same(s_row, slot_row[0]) + same(s_row, slot_row[1])).astype(jnp.bfloat16)
    s_col = lax.broadcasted_iota(jnp.int32, (rows, slots), 1).astype(jnp.float32)
    pick = [same(s_col, slot_col[k]).astype(jnp.bfloat16) for k in (0, 1)]
    i_dst = lax.broadcasted_iota(jnp.int32, (slots, slots), 0)
    i_src = lax.broadcasted_iota(jnp.int32, (slots, slots), 1)
    from_row = lax.div(lax.rem(i_dst, block), capacity) * block + lax.div(i_dst, block) * capacity + lax.rem(i_dst, capacity)
    swap = jnp.where(i_src == from_row, 1.0, 0.0).astype(jnp.bfloat16)

    def norm(summed, n):
        center = summed - jnp.mean(summed, axis=-1, keepdims=True)
        spread_ = jnp.mean(center * center, axis=-1, keepdims=True)
        scaled = center * lax.rsqrt(spread_ + LN_EPS) * gain_ref[n : n + 1, :] + bias_ref[n : n + 1, :]
        return scaled.astype(jnp.bfloat16)

    mixed = proj[y].astype(jnp.float32)
    for way in (1, -1, 2):
        source = y_side[2 if way == 2 else -way]
        arrive(("proj", way), proj_in.at[source])
        mixed = mixed + proj_in[source].astype(jnp.float32)
    normed[...] = norm(ALPHA * res_ref[...].astype(jnp.float32) + mixed, 0)
    tokens[y] = normed[...]

    def rows_at(n):
        return pl.ds(pl.multiple_of(n * block, block), block)

    def exchange(tag, q, axis, outgoing, incoming):
        here, size = (z, rows_z) if axis == "z" else (w, group)
        for d in range(1, size):
            there = turn(here, d, size)
            target = {"sp": there * group + w} if axis == "z" else {"sp": z * group + there}
            begin((tag, q, d), outgoing.at[rows_at(there), span(q)], incoming.at[rows_at(here), span(q)], target)
        incoming[rows_at(here), span(q)] = outgoing[rows_at(here), span(q)]

    def exchanged(tag, q, axis, incoming):
        here, size = (z, rows_z) if axis == "z" else (w, group)
        for d in range(1, size):
            arrive((tag, q, d), incoming.at[rows_at(turn(here, -d, size)), span(q)])

    def moved(matrix, value):
        return jnp.dot(matrix, value, preferred_element_type=jnp.float32).astype(jnp.bfloat16)

    def act(g, u):
        return (g / (1.0 + jnp.exp(-g)) * u).astype(jnp.bfloat16)

    def d0(q):
        out_z[:, span_of(q)] = moved(place, normed[:, span_of(q)])
        exchange("dz", q, "z", out_z, in_z)

    def d1(q):
        exchanged("dz", q, "z", in_z)
        out_x[:, span_of(q)] = moved(swap, in_z[:, span_of(q)])
        exchange("dx", q, "x", out_x, rows_all.at[y])

    def d2(q):
        exchanged("dx", q, "x", rows_all.at[y])
        for way in ways:
            begin(("dy", q, way), rows_all.at[y, :, span(q)], rows_all.at[y, :, span(q)], to_y[way])

    row_half = halves(slots)

    def d3(q):
        for way in ways:
            side = y_side[-way]
            arrive(("dy", q, way), rows_all.at[side, :, span(q)])
            half = rows_all.at[side, row_half[way], span(q)]
            begin(("dy", q, "far", way), half, half, to_y[way])

    def d4(q):
        for way in ways:
            arrive(("dy", q, "far", way), rows_all.at[y_side[2], row_half[way], span(q)])
        xs = rows_all[:, :, span_of(q)].reshape(tp * slots, cols)
        if q == 0:
            loads[4].wait()
            loads[5].wait()
        g = jnp.dot(xs, wg[span_of(q), :], preferred_element_type=jnp.float32)
        u = jnp.dot(xs, wu[span_of(q), :], preferred_element_type=jnp.float32)
        gate[...] = g if q == 0 else gate[...] + g
        up[...] = u if q == 0 else up[...] + u

    def shared_in():
        for way in (1, -1, 2):
            arrive(("tok", way), tokens.at[y_side[2 if way == 2 else -way]])
        loads[2].wait()
        loads[3].wait()
        loads[6].wait()
        xs = tokens[...].reshape(tp * rows, width)
        g = jnp.dot(xs, sg[...], preferred_element_type=jnp.float32)
        u = jnp.dot(xs, su[...], preferred_element_type=jnp.float32)
        shared_hidden[...] = act(g, u)
        s = jnp.dot(shared_hidden[...], sd[...], preferred_element_type=jnp.float32)
        part[...] = s.astype(jnp.bfloat16).reshape(tp, rows, width)

    piece = halves(rows)

    def shared_far():
        for way in ways:
            begin(("sh", "far", way), part.at[y_side[2], piece[way]], part_far.at[0 if way == 1 else 1], to_y[way])

    def shared_pass():
        for way in ways:
            n = 0 if way == 1 else 1
            arrive(("sh", "far", way), part_far.at[n])
            mine = part.at[y_side[way], piece[way]]
            mine[...] = (mine[...].astype(jnp.float32) + part_far[n].astype(jnp.float32)).astype(jnp.bfloat16)
            begin(("sh", "near", way), part.at[y_side[way]], part_in.at[n], to_y[way])

    def shared_out():
        acc = part[y].astype(jnp.float32)
        for way in ways:
            n = 0 if way == 1 else 1
            arrive(("sh", "near", way), part_in.at[n])
            acc = acc + part_in[n].astype(jnp.float32)
        total[...] = ALPHA * normed[...].astype(jnp.float32) + acc.astype(jnp.bfloat16).astype(jnp.float32)

    def e0(q):
        acc = jnp.dot(hidden_in[0], wd[0, :, span_of(q)], preferred_element_type=jnp.float32)
        for j in range(1, tp):
            acc = acc + jnp.dot(hidden_in[j], wd[j, :, span_of(q)], preferred_element_type=jnp.float32)
        back_x[:, span_of(q)] = acc.astype(jnp.bfloat16)
        exchange("rx", q, "x", back_x, in_bx)

    def e1(q):
        exchanged("rx", q, "x", in_bx)
        back_z[:, span_of(q)] = moved(swap, in_bx[:, span_of(q)])
        exchange("rz", q, "z", back_z, in_bz)

    def e2(q):
        exchanged("rz", q, "z", in_bz)
        got = in_bz[:, span_of(q)]
        routed = [
            jnp.dot(pick[k], got, preferred_element_type=jnp.float32) * rw_ref[:, k : k + 1]
            for k in (0, 1)
        ]
        total[:, span_of(q)] = total[:, span_of(q)] + (routed[0] + routed[1])

    d0(0)
    for way in every_way:
        begin(("tok", way), tokens.at[y], tokens.at[y], to_y[way])
    for q in range(1, chunks):
        d0(q)

    def pipeline(stages, extra):
        for step in range(chunks + len(stages) - 1):
            for s, stage in enumerate(stages):
                if 0 <= step - s < chunks:
                    stage(step - s)
            if step in extra:
                extra[step]()

    pipeline((d1, d2, d3, d4), {0: shared_in, chunks: shared_far, chunks + 1: lambda: relay_down(chunks - 1)})
    hidden[...] = act(gate[...], up[...]).reshape(tp, slots, hidden.shape[2])
    for way in every_way:
        begin(("hid", way), hidden.at[y_side[way]], hidden_in.at[y], to_y[way])
    hidden_in[y] = hidden[y]
    shared_pass()
    loads[0].wait()
    for q in range(chunks):
        relayed_down(q)
    for way in (1, -1, 2):
        arrive(("hid", way), hidden_in.at[y_side[2 if way == 2 else -way]])
    pipeline((e0, e1, e2), {0: shared_out})
    out_ref[...] = norm(total[...], 1)
    for job in started:
        job.wait_send()


def layer(head_offset, query_rows, key_rows, value_rows, residual, routing, route_weight,
          norm_gain, norm_bias, w_out, w_exp_gate, w_exp_up, w_exp_down,
          w_shared_gate, w_shared_up, w_shared_down):
    rows, width = residual.shape
    q_rows, q_width = query_rows.shape
    dh = key_rows.shape[1]
    heads = head_offset.shape[0]
    tp = lax.axis_size("tp")
    sp = lax.axis_size("sp")
    rows_z, rows_x = cross(sp)
    capacity = 2
    slots = sp * capacity
    ff = w_exp_gate.shape[2]
    bf16, f32 = jnp.bfloat16, jnp.float32
    vmem = pl.BlockSpec(memory_space=pltpu.VMEM)
    hbm = pl.BlockSpec(memory_space=pl.ANY)
    kv = pltpu.VMEM((rows_z, rows_x, 2, q_rows, dh), bf16)
    routed = pltpu.VMEM((slots, width), bf16)
    scratch = [
        kv,
        kv,
        pltpu.VMEM((q_rows, q_width), f32),
        pltpu.VMEM((q_rows, q_width), f32),
        pltpu.VMEM((heads, q_rows, dh), f32),
        pltpu.VMEM(w_out.shape, bf16),
        pltpu.VMEM((width, ff), bf16),
        pltpu.VMEM((width, ff), bf16),
        pltpu.VMEM((tp, ff, width), bf16),
        pltpu.VMEM(w_shared_gate.shape, bf16),
        pltpu.VMEM(w_shared_up.shape, bf16),
        pltpu.VMEM(w_shared_down.shape, bf16),
        pltpu.VMEM((tp, rows, width), bf16),
        pltpu.VMEM((tp, rows, width), bf16),
        pltpu.VMEM((rows, width), bf16),
        pltpu.VMEM((tp, rows, width), bf16),
        routed,
        routed,
        routed,
        pltpu.VMEM((tp, slots, width), bf16),
        pltpu.VMEM((tp * slots, ff), f32),
        pltpu.VMEM((tp * slots, ff), f32),
        pltpu.VMEM((tp * rows, w_shared_gate.shape[1]), bf16),
        pltpu.VMEM((tp, slots, ff), bf16),
        pltpu.VMEM((tp, slots, ff), bf16),
        pltpu.VMEM((tp, rows, width), bf16),
        pltpu.VMEM((2, rows // 2, width), bf16),
        pltpu.VMEM((2, rows, width), bf16),
        routed,
        routed,
        routed,
        routed,
        pltpu.VMEM((rows, width), f32),
        pltpu.SemaphoreType.DMA((288,)),
        pltpu.SemaphoreType.DMA((288,)),
        pltpu.SemaphoreType.DMA((9,)),
    ]
    return pl.pallas_call(
        functools.partial(layer_kernel, rows_z, rows_x, 4, capacity),
        out_shape=jax.ShapeDtypeStruct((rows, width), bf16),
        in_specs=[pl.BlockSpec(memory_space=pltpu.SMEM)] + [vmem] * 8 + [hbm] * 7,
        out_specs=vmem,
        scratch_shapes=scratch,
        compiler_params=pltpu.CompilerParams(
            collective_id=0, has_side_effects=True, vmem_limit_bytes=67043328
        ),
        name="layer",
    )(head_offset, query_rows, key_rows, value_rows, residual, routing, route_weight,
      norm_gain, norm_bias, w_out, w_exp_gate, w_exp_up, w_exp_down,
      w_shared_gate, w_shared_up, w_shared_down)


def per_device(
    residual,
    query_rows,
    key_rows,
    value_rows,
    head_offset,
    w_out,
    norm_gain,
    norm_bias,
    routing,
    route_weight,
    w_exp_gate,
    w_exp_up,
    w_exp_down,
    w_shared_gate,
    w_shared_up,
    w_shared_down,
):
    return layer(
        head_offset, query_rows, key_rows, value_rows, residual, routing, route_weight,
        norm_gain, norm_bias, w_out, w_exp_gate, w_exp_up, w_exp_down,
        w_shared_gate, w_shared_up, w_shared_down,
    )


def solution(mesh):
    placed = (
        P(("sp", "tp"), None),
        P("sp", "tp"),
        P("sp", "tp"),
        P("sp", "tp"),
        P("tp"),
        P("tp", None),
        P(),
        P(),
        P(("sp", "tp"), None),
        P(("sp", "tp"), None),
        P("sp", None, "tp"),
        P("sp", None, "tp"),
        P("sp", "tp", None),
        P(None, "tp"),
        P(None, "tp"),
        P("tp", None),
    )
    return jax.shard_map(
        per_device, mesh=mesh, in_specs=placed, out_specs=P(("sp", "tp"), None), check_vma=False
    )
```

time: 271 us -> 119 us (0.44)
  waiting for transfers between devices: 130 us -> 0 us
  Pallas kernels: 4.1 us -> 115 us
  blocking collectives: 59.5 us -> 0 us
  starting transfers between devices: 25.5 us -> 0 us
  between operations: 13.6 us -> 0.01 us
  local copies, waits for them, and re-layouts: 16.6 us -> 3.63 us
  matrix products: 12.8 us -> 0 us
  other arithmetic: 8.02 us -> 0 us
    pallas_call x1, Pallas kernels: 4.1 us -> 115 us  [layer(): pl.pallas_call(functools.partial(layer_kernel, rows_z, rows_x, 4, capacit...]
    all_gather x1 -> x0, waiting for transfers between devices: 81.3 us -> none  [in_one_piece(): whole, at, done = (lax.all_gather(both, axis, axis=dim, tiled=True), 0, [])]
    all_to_all x2 -> x0, blocking collectives: 59.5 us -> none  [the longest x1 31 us: per_device(): lax.all_to_all(outgoing, 'sp', split_axis=0, concat_axis=0, tiled=True)]
    all_to_all x5 -> x0, waiting for transfers between devices: 48.3 us -> none  [the longest x3 31.9 us: summed_on_arrival(): blocks = lax.all_to_all(split_up(array, dim, peers), axis, 0, 0, tiled=True)]
    all_to_all x5 -> x0, starting transfers between devices: 25.5 us -> none  [the longest x3 12.3 us: summed_on_arrival(): blocks = lax.all_to_all(split_up(array, dim, peers), axis, 0, 0, tiled=True)]
    dot_general x5 -> x0, matrix products: 12.8 us -> none  [the longest x1 4.29 us: per_device(): jnp.einsum('aecf,efd->aecd', hidden, w_exp_down, preferred_element_type=j...]
    slice x3 -> x0, local copies, waits for them, and re-layouts: 5.29 us -> none  [the longest x1 4.46 us: in_one_piece(): done.append(lax.slice_in_dim(whole, at, at + a.shape[along], axis=along))]
    reduce_sum x9 -> x0, other arithmetic: 4.17 us -> none  [the longest x3 2.54 us: summed_on_arrival(): return jnp.sum(blocks.astype(jnp.float32), axis=0)]
  transfers between devices with their start and end apart: 6 -> 0, of which waited for: 5 -> 0; matrix products, arithmetic and copies ran while one was open for 8% -> 0% of each run, Pallas kernels for 0% -> 0%
where the time goes in v4:
time: 119 us
  Pallas kernels  115 us (97%)
  local copies, waits for them, and re-layouts  3.63 us (3%)
    pallas_call x1, Pallas kernels, layer(): pl.pallas_call(functools.partial(layer_kernel, rows_z, rows_x, 4, capacit...  115 us
    unnamed x5, local copies, waits for them, and re-layouts  3.63 us

profile of v4, /device:TPU:1, one launch (start us, length us, event | category | flops | bytes accessed | tf_op | source)
XLA Modules:
  0.0 118.9 jit_solution(11464817713366659389)
XLA Ops:
  0.0 0.0 copy-start
  0.0 1.4 %copy.17.route_ref = s32[32,2]{1,0:T(8,128)} copy(s32[32,2]{0,1:T(2,128)} %param.24) | data formatting | bytes 512 | tf_op args[8]
  1.4 0.0 copy-done
  1.4 0.7 copy.18.rw_ref
  2.1 115.2 %layer.1 = bf16[32,2048]{1,0:T(8,128)(2,1)} custom-call(f32[2]{0:T(128)} %off_ref.1, bf16[128,256]{1,0:T(8,128)(2,1)} %q_ref.1, bf16[128,128]{1,0:T(8,128)(2,1)} %k_ref.1, bf16[128,128]{1,0:T(8,128)(2,1)} %v_ref.1, bf16[32,2048]{1,0:T(8,128)(2,1)} %res_ref.1, s32[32,2]{1,0:T(8,128)} %copy.17.route_ref, f32[32,2]{1,0:T(8,128)} %copy.18.rw_ref, ...), custom_call_target="tpu_custom_call" | custom-call | tf_op jit(solution)/shard_map/layer/pallas_call | solution.py:553
  117.3 1.6 %copy.20 = bf16[32,2048]{1,0:T(8,128)(2,1)} copy(bf16[32,2048]{1,0:T(8,128)(2,1)} %layer.1) | data formatting | bytes 262144
Async XLA Ops:
  0.0 1.4 %copy-start = (f32[32,2]{0,1:T(2,128)S(1)}, f32[32,2]{0,1:T(2,128)}, u32[]{:S(2)}) copy-start(f32[32,2]{0,1:T(2,128)} %param.25) | copy-start | bytes 772
